TPU v7x, 128 devices: a whole 4x4x4 slice. The times are simulated.
128 devices in a mesh: dp: 4 (over x), kv: 16 (over z, y), tp: 2 (over core).
Axes of the slice: x: 4, y: 4, z: 4, core: 2. Of those that a mesh axis runs over, the one named last changes fastest.
Arguments:
- tokens: bfloat16 [512, 2048], P('dp', 'kv'), may hold values from -18 to 18
- mix_gain: float32 [2048], P('kv'), may hold values from 0.1 to 1.9
- w_query: bfloat16 [2048, 1024], P('kv', 'tp'), may hold values from -0.125 to 0.125
- w_key: bfloat16 [2048, 1024], P('kv', 'tp'), may hold values from -0.125 to 0.125
- w_value: bfloat16 [2048, 2048], P('kv', 'tp'), may hold values from -0.125 to 0.125
- w_outgate: bfloat16 [2048, 2048], P('kv', 'tp'), may hold values from -0.125 to 0.125
- w_gates: bfloat16 [2048, 16], replicated, may hold values from -0.25 to 0.25
- forget_bias: float32 [8], P('tp'), may hold values from -1 to 3
- memory: float32 [512, 8, 128, 256], P(('dp', 'kv'), 'tp'), may hold values from -4 to 4
- normalizer: float32 [512, 8, 128], P(('dp', 'kv'), 'tp'), may hold values from -4 to 4
- stabilizer: float32 [512, 8], P(('dp', 'kv'), 'tp'), may hold values from -4 to 4
- head_gain: float32 [8, 256], P('tp'), may hold values from 0.1 to 1.9
- w_out: bfloat16 [2048, 2048], P('tp', 'kv'), may hold values from -0.125 to 0.125
- mlp_gain: float32 [2048], replicated, may hold values from 0.1 to 1.9
- w_gate: bfloat16 [2048, 5632], P(None, ('kv', 'tp')), may hold values from -0.125 to 0.125
- w_up: bfloat16 [2048, 5632], P(None, ('kv', 'tp')), may hold values from -0.125 to 0.125
- w_down: bfloat16 [5632, 2048], P(('kv', 'tp')), may hold values from -0.15625 to 0.15625
Outputs:
- mixed_out: bfloat16 [512, 2048], P('dp', ('kv', 'tp'))
- new_memory: float32 [512, 8, 128, 256], P(('dp', 'kv'), 'tp')
- new_normalizer: float32 [512, 8, 128], P(('dp', 'kv'), 'tp')
- new_stabilizer: float32 [512, 8], P(('dp', 'kv'), 'tp')
All inputs are finite; a program needn't handle non-finite values.
Results may differ from a plain program's by a relative error of at most 0.02.
Values may be sent and summed in bfloat16 or wider, within the bound.
A program may use at most 64 MiB of HBM per device.

v0:
```python
import jax
import jax.numpy as jnp
from jax import lax
from jax.sharding import PartitionSpec as P

QK = 128
VD = 256


EPSILON = 1e-06


def cut_along(value, dim, devices):
    before, after = (value.shape[:dim], value.shape[dim + 1 :])
    return jnp.moveaxis(value.reshape(*before, devices, -1, *after), dim, 0)


def sum_at_owner(value, axis, dim):
    devices = lax.axis_size(axis)
    blocks = lax.all_to_all(cut_along(value, dim, devices), axis, 0, 0, tiled=True)
    return jnp.sum(blocks.astype(jnp.float32), axis=0)


def side_by_side(arrays, axis, dim, along):
    both = jnp.concatenate(arrays, axis=along)
    whole, at, gathered = (sum_at_owner(both, axis, dim), 0, [])
    for a in arrays:
        gathered.append(lax.slice_in_dim(whole, at, at + a.shape[along], axis=along))
        at += a.shape[along]
    return tuple(gathered)


def from_everyone(value, axis):
    devices = lax.axis_size(axis)
    return lax.all_to_all(
        jnp.broadcast_to(value[None], (devices, *value.shape)), axis, 0, 0, tiled=True
    )


def joined_along(blocks, dim):
    shape = list(blocks.shape[1:])
    shape[dim] *= blocks.shape[0]
    return jnp.moveaxis(blocks, 0, dim).reshape(shape)


def gathered_copies(value, axis, dim):
    blocks = from_everyone(value, axis)
    return joined_along(blocks, dim)


def over_copies(value, axis):
    everything = from_everyone(value, axis)
    return jnp.sum(everything.astype(jnp.float32), axis=0)


def front_half(
    query_sum,
    key_sum,
    gate_sum,
    square_sum,
    model_width,
    forget_bias,
    memory,
    normalizer,
    stabilizer,
):
    local_heads = forget_bias.shape[0]
    seq_rows = query_sum.shape[0]
    inverse = lax.rsqrt(square_sum / model_width + EPSILON)
    query_rows = (query_sum * inverse).astype(jnp.bfloat16)
    key_rows = (key_sum * (inverse * QK ** (-0.5))).astype(jnp.bfloat16)
    gate_pre = gate_sum * inverse
    input_pre = gate_pre[:, :local_heads]
    log_forget = jax.nn.log_sigmoid(gate_pre[:, local_heads:] + forget_bias)
    new_stabilizer = jnp.maximum(log_forget + stabilizer, input_pre)
    forget_scale = jnp.exp(log_forget + stabilizer - new_stabilizer)
    input_scale = jnp.exp(input_pre - new_stabilizer)
    query_heads = query_rows.astype(jnp.float32).reshape(seq_rows, local_heads, QK)
    key_heads = key_rows.astype(jnp.float32).reshape(seq_rows, local_heads, QK)
    new_normalizer = forget_scale[..., None] * normalizer + input_scale[..., None] * key_heads
    denominator = jnp.sum(query_heads * new_normalizer, axis=2)
    carried = jnp.einsum("bhd,bhde->bhe", query_heads, memory)
    query_key = jnp.sum(query_heads * key_heads, axis=2)
    return (
        inverse,
        new_stabilizer,
        forget_scale,
        input_scale,
        key_heads,
        new_normalizer,
        denominator,
        carried,
        query_key,
    )


def back_half(value_sum, outgate_sum, front_state, memory, head_gain):
    (
        inverse,
        new_stabilizer,
        forget_scale,
        input_scale,
        key_heads,
        new_normalizer,
        denominator,
        carried,
        query_key,
    ) = front_state
    seq_rows, local_heads = forget_scale.shape
    value_rows = (value_sum * inverse).astype(jnp.bfloat16)
    outgate = (outgate_sum * inverse).astype(jnp.bfloat16)
    value_heads = value_rows.astype(jnp.float32).reshape(seq_rows, local_heads, VD)
    new_memory = (
        forget_scale[..., None, None] * memory
        + (input_scale[..., None] * key_heads)[..., None] * value_heads[:, :, None, :]
    )
    numerator = (
        forget_scale[..., None] * carried + (input_scale * query_key)[..., None] * value_heads
    )
    head_out = numerator / jnp.maximum(jnp.abs(denominator), 1.0)[..., None]
    normed = (
        head_out
        * lax.rsqrt(jnp.mean(head_out * head_out, axis=2, keepdims=True) + EPSILON)
        * head_gain
    )
    mixed_heads = (
        normed.reshape(seq_rows, local_heads * VD) * jax.nn.sigmoid(outgate.astype(jnp.float32))
    ).astype(jnp.bfloat16)
    return (new_memory, mixed_heads)


def body(
    tokens,
    mix_gain,
    w_query,
    w_key,
    w_value,
    w_outgate,
    w_gates,
    forget_bias,
    memory,
    normalizer,
    stabilizer,
    head_gain,
    w_out,
    mlp_gain,
    w_gate,
    w_up,
    w_down,
):
    activations = tokens.astype(jnp.float32)
    block_cols = tokens.shape[1]
    model_width = block_cols * lax.axis_size("kv")
    square_part = jnp.sum(activations * activations, axis=1, keepdims=True)
    scaled = (activations * mix_gain).astype(jnp.bfloat16)
    local_heads = forget_bias.shape[0]
    total_heads = w_gates.shape[1] // 2
    head_start = lax.axis_index("tp") * local_heads
    gate_rows = lax.dynamic_slice_in_dim(w_gates, lax.axis_index("kv") * block_cols, block_cols, 0)
    gate_cols = jnp.concatenate(
        [
            lax.dynamic_slice_in_dim(gate_rows, head_start, local_heads, 1),
            lax.dynamic_slice_in_dim(gate_rows, total_heads + head_start, local_heads, 1),
        ],
        axis=1,
    )
    query_part = jnp.dot(scaled, w_query, preferred_element_type=jnp.float32)
    key_part = jnp.dot(scaled, w_key, preferred_element_type=jnp.float32)
    value_part = jnp.dot(scaled, w_value, preferred_element_type=jnp.float32)
    outgate_part = jnp.dot(scaled, w_outgate, preferred_element_type=jnp.float32)
    gate_part = jnp.dot(scaled, gate_cols, preferred_element_type=jnp.float32)
    query_sum, key_sum, value_sum, outgate_sum, gate_sum, square_sum = side_by_side(
        (
            query_part.astype(jnp.bfloat16),
            key_part.astype(jnp.bfloat16),
            value_part.astype(jnp.bfloat16),
            outgate_part.astype(jnp.bfloat16),
            gate_part.astype(jnp.bfloat16),
            square_part.astype(jnp.bfloat16),
        ),
        "kv",
        0,
        1,
    )
    front_state = front_half(
        query_sum,
        key_sum,
        gate_sum,
        square_sum,
        model_width,
        forget_bias,
        memory,
        normalizer,
        stabilizer,
    )
    new_memory, mixed_heads = back_half(value_sum, outgate_sum, front_state, memory, head_gain)
    new_stabilizer = front_state[1]
    new_normalizer = front_state[5]
    branch_part = jnp.dot(
        gathered_copies(mixed_heads, "kv", 0), w_out, preferred_element_type=jnp.float32
    )
    branch = over_copies(branch_part.astype(jnp.bfloat16), "tp").astype(jnp.float32)
    residual = (activations + branch).astype(jnp.bfloat16)
    gathered = gathered_copies(residual, "kv", 1)
    gathered_float = gathered.astype(jnp.float32)
    inverse_two = lax.rsqrt(
        jnp.mean(gathered_float * gathered_float, axis=1, keepdims=True) + EPSILON
    )
    mlp_in = (gathered_float * inverse_two * mlp_gain).astype(jnp.bfloat16)
    gate_value = jnp.dot(mlp_in, w_gate, preferred_element_type=jnp.float32)
    up_value = jnp.dot(mlp_in, w_up, preferred_element_type=jnp.float32)
    hidden = (jax.nn.silu(gate_value) * up_value).astype(jnp.bfloat16)
    down_part = jnp.dot(hidden, w_down, preferred_element_type=jnp.float32)
    out_cols = block_cols // lax.axis_size("tp")
    own_residual = lax.dynamic_slice_in_dim(
        residual.astype(jnp.float32), lax.axis_index("tp") * out_cols, out_cols, 1
    )
    summed = sum_at_owner(down_part.astype(jnp.bfloat16), ("kv", "tp"), 1)
    mixed_out = (summed + own_residual).astype(jnp.bfloat16)
    return (mixed_out, new_memory, new_normalizer, new_stabilizer)


def solution(mesh):
    in_specs = (
        P("dp", "kv"),
        P("kv"),
        P("kv", "tp"),
        P("kv", "tp"),
        P("kv", "tp"),
        P("kv", "tp"),
        P(),
        P("tp"),
        P(("dp", "kv"), "tp", None, None),
        P(("dp", "kv"), "tp", None),
        P(("dp", "kv"), "tp"),
        P("tp", None),
        P("tp", "kv"),
        P(),
        P(None, ("kv", "tp")),
        P(None, ("kv", "tp")),
        P(("kv", "tp"), None),
    )
    out_specs = (
        P("dp", ("kv", "tp")),
        P(("dp", "kv"), "tp", None, None),
        P(("dp", "kv"), "tp", None),
        P(("dp", "kv"), "tp"),
    )
    return jax.shard_map(body, mesh=mesh, in_specs=in_specs, out_specs=out_specs, check_vma=False)
```

profile of v0, /device:TPU:1, one launch (start us, length us, event | category | flops | bytes accessed | tf_op | source)
XLA Modules:
  0.0 87.8 jit_solution(3687271985800106806)
XLA Ops:
  0.6 0.0 copy-start
  0.6 0.0 copy-start.8
  0.7 0.0 copy-start.9
  0.7 0.0 copy-start.5
  0.7 0.9 %fusion.14 = bf16[128]{0:T(256)(128)(2,1)S(1)} fusion(bf16[128,128]{1,0:T(8,128)(2,1)} %param.17), kind=kLoop, calls=%fused_computation.31 | loop fusion | flops 49024 | bytes 33024 | tf_op jit(solution)/shard_map/reduce_sum | solution.py:154
  1.6 0.9 fusion.46
  2.5 0.9 %convolution_convert_fusion.6 = bf16[128,8]{0,1:T(8,128)(2,1)S(1)} fusion(bf16[128,128]{1,0:T(8,128)(2,1)} %param.17, f32[128]{0:T(128)} %param.18, bf16[128,4]{0,1:T(4,128)(2,1)S(1)} %get-tuple-element.32, bf16[128,4]{0,1:T(4,128)(2,1)S(1)} %get-tuple-element.31), kind=kOutput, calls=%fused_computation.14 | convolution fusion | flops 316416 | bytes 37376 | tf_op jit(solution)/shard_map/dot_general | solution.py:171
  3.4 0.1 copy.102
  3.5 0.2 convert_element_type.131
  3.7 1.1 %fusion.2 = bf16[16,8,512]{2,1,0:T(8,128)(2,1)S(1)} fusion(bf16[128,512]{1,0:T(8,128)(2,1)} %param.19, bf16[128,128]{1,0:T(8,128)(2,1)} %param.17, f32[128]{0:T(128)} %param.18), kind=kOutput, calls=%fused_computation.9 | convolution fusion | flops 16891904 | bytes 295424 | tf_op jit(solution)/shard_map/dot_general | solution.py:167
  4.9 1.1 %fusion.3 = bf16[16,8,512]{2,1,0:T(8,128)(2,1)S(1)} fusion(bf16[128,512]{1,0:T(8,128)(2,1)} %param.20, bf16[128,128]{1,0:T(8,128)(2,1)} %param.17, f32[128]{0:T(128)} %param.18), kind=kOutput, calls=%fused_computation.10 | convolution fusion | flops 16891904 | bytes 295424 | tf_op jit(solution)/shard_map/dot_general | solution.py:168
  6.0 1.2 %fusion = bf16[16,8,1024]{2,1,0:T(8,128)(2,1)S(1)} fusion(bf16[128,1024]{1,0:T(8,128)(2,1)} %param.21, bf16[128,128]{1,0:T(8,128)(2,1)} %param.17, f32[128]{0:T(128)} %param.18), kind=kOutput, calls=%fused_computation.5 | convolution fusion | flops 33734656 | bytes 557568 | tf_op jit(solution)/shard_map/dot_general | solution.py:169
  7.2 1.2 %fusion.1 = bf16[16,8,1024]{2,1,0:T(8,128)(2,1)S(1)} fusion(bf16[128,1024]{1,0:T(8,128)(2,1)} %param.22, bf16[128,128]{1,0:T(8,128)(2,1)} %param.17, f32[128]{0:T(128)} %param.18), kind=kOutput, calls=%fused_computation.6 | convolution fusion | flops 33734656 | bytes 557568 | tf_op jit(solution)/shard_map/dot_general | solution.py:170
  8.4 0.0 copy-start.7
  8.4 1.1 %concatenate.23 = bf16[16,8,3081]{2,1,0:T(8,128)(2,1)} concatenate(bf16[16,8,512]{2,1,0:T(8,128)(2,1)S(1)} %fusion.2, bf16[16,8,512]{2,1,0:T(8,128)(2,1)S(1)} %fusion.3, bf16[16,8,1024]{2,1,0:T(8,128)(2,1)S(1)} %fusion, bf16[16,8,1024]{2,1,0:T(8,128)(2,1)S(1)} %fusion.1, bf16[16,8,8]{2,1,0:T(8,128)(2,1)S(1)} %bitcast.60, bf16[16,8,1]{2,1,0:T(8,128)(2,1)S(1)} %convert_element_type.131), dimensions={2} | concatenate | bytes 1577472 | tf_op jit(solution)/shard_map/concatenate | solution.py:25
  9.5 0.0 copy-start.4
  9.5 0.0 copy-start.1
  9.5 8.7 %all-to-all-start = ((bf16[16,8,3081]{2,1,0:T(8,128)(2,1)}), bf16[16,8,3081]{2,1,0:T(8,128)(2,1)S(1)}, u32[]{:S(2)}, u32[]{:S(2)}) async-start(bf16[16,8,3081]{2,1,0:T(8,128)(2,1)} %concatenate.23), calls=%async_computation | async-start | bytes 1638400 | tf_op jit(solution)/shard_map/all_to_all | solution.py:20
  18.2 0.0 copy-done.8
  18.2 0.1 copy.87
  18.3 13.5 %all-to-all-done = bf16[16,8,3081]{2,1,0:T(8,128)(2,1)S(1)} async-done(((bf16[16,8,3081]{2,1,0:T(8,128)(2,1)}), bf16[16,8,3081]{2,1,0:T(8,128)(2,1)S(1)}, u32[]{:S(2)}, u32[]{:S(2)}) %all-to-all-start) | async-done | bytes 788768 | tf_op jit(solution)/shard_map/all_to_all | solution.py:20
  31.8 0.1 convert_reduce_fusion
  31.9 0.2 fusion.38
  32.1 0.1 slice_multiply_fusion.5
  32.2 0.1 fusion.18
  32.2 0.0 copy-done.9
  32.2 0.1 subtract_exponential_fusion.1
  32.4 0.1 copy.88
  32.4 0.1 fusion.44
  32.5 0.0 copy-done.5
  32.5 0.7 fusion.21
  33.2 0.1 copy.91
  33.3 0.1 copy.93
  33.4 0.0 copy-start.6
  33.4 2.6 %fusion.25 = f32[8,4,1,256]{3,2,1,0:T(1,128)S(1)} fusion(f32[8,4,128,256]{3,2,1,0:T(8,128)} %param.25, bf16[8,4,128,1]{2,0,1,3:T(8,128)(2,1)S(1)} %get-tuple-element.28), kind=kOutput, calls=%fused_computation.53 | convolution fusion | flops 2097152 | bytes 4235264 | tf_op jit(solution)/shard_map/bhd,bhde->bhe/dot_general | solution.py:82
  36.0 0.2 multiply_reduce_fusion.1
  36.2 0.0 copy-done.7
  36.2 0.1 multiply_multiply_fusion
  36.3 0.1 multiply_convert_fusion
  36.4 11.2 %all_to_all.25 = bf16[16,8,1024]{2,1,0:T(8,128)(2,1)S(1)} all-to-all(bf16[16,8,1024]{2,1,0:T(8,128)(2,1)S(1)} %broadcast_in_dim.6), channel_id=1, replica_groups=mesh['dp'=4,'kv'=16,'tp'=2] {'kv'}, dimensions={0} | all-to-all | bytes 524288 | tf_op jit(solution)/shard_map/all_to_all | solution.py:35
  47.7 0.0 copy-done.4
  47.7 0.2 convolution_convert_fusion.5
  47.9 5.8 %all_to_all.26 = bf16[2,128,128]{2,1,0:T(8,128)(2,1)S(1)} all-to-all(bf16[2,128,128]{2,1,0:T(8,128)(2,1)S(1)} %broadcast_in_dim.7), channel_id=1, replica_groups=mesh['dp'=4,'kv'=16,'tp'=2] {'tp'}, dimensions={0} | all-to-all | bytes 131072 | tf_op jit(solution)/shard_map/all_to_all | solution.py:35
  53.7 0.0 copy-done.1
  53.7 0.1 copy.94
  53.9 0.1 broadcast_in_dim.8
  54.0 13.4 %all_to_all.27 = bf16[16,128,128]{1,2,0:T(8,128)(2,1)S(1)} all-to-all(bf16[16,128,128]{1,2,0:T(8,128)(2,1)S(1)} %broadcast_in_dim.8), channel_id=1, replica_groups=mesh['dp'=4,'kv'=16,'tp'=2] {'kv'}, dimensions={0} | all-to-all | bytes 1048576 | tf_op jit(solution)/shard_map/all_to_all | solution.py:35
  67.3 0.3 multiply_reduce_fusion
  67.6 0.0 copy-done.6
  67.6 0.3 fusion.6
  68.0 0.0 copy-done.2
  68.0 0.3 fusion.47
  68.3 0.0 copy-done
  68.4 0.0 copy-done.3
  68.4 0.7 convolution_convert_fusion
  69.0 1.0 %copy.95 = bf16[128,2048]{0,1:T(8,128)(2,1)} copy(bf16[128,2048]{1,0:T(8,128)(2,1)S(1)} %convolution_convert_fusion) | data formatting | bytes 1048576 | tf_op jit(solution)/shard_map/convert_element_type | solution.py:218
  70.0 5.3 %all-to-all-start.4 = ((bf16[32,128,64]{1,2,0:T(8,128)(2,1)}), bf16[32,128,64]{1,2,0:T(8,128)(2,1)S(1)}, u32[]{:S(2)}, u32[]{:S(2)}) async-start(bf16[32,128,64]{1,2,0:T(8,128)(2,1)} %bitcast.16), calls=%async_computation.4 | async-start | bytes 1048576 | tf_op jit(solution)/shard_map/all_to_all | solution.py:20
  75.3 0.7 copy.99
  76.0 4.0 %multiply_add_fusion = f32[8,4,128,256]{3,2,1,0:T(8,128)} fusion(f32[8,4,128,256]{3,2,1,0:T(8,128)} %param.25, f32[8,4,256]{2,1,0:T(4,128)S(1)} %copy.97, f32[8,4,128]{2,1,0:T(4,128)S(1)} %get-tuple-element.25, f32[8,4]{1,0:T(8,128)S(1)} %get-tuple-element.26), kind=kLoop, calls=%fused_computation | loop fusion | flops 3145728 | bytes 8437888 | tf_op jit(solution)/shard_map/add | solution.py:114
  79.9 6.9 %all-to-all-done.4 = bf16[32,128,64]{1,2,0:T(8,128)(2,1)S(1)} async-done(((bf16[32,128,64]{1,2,0:T(8,128)(2,1)}), bf16[32,128,64]{1,2,0:T(8,128)(2,1)S(1)}, u32[]{:S(2)}, u32[]{:S(2)}) %all-to-all-start.4) | async-done | bytes 524320 | tf_op jit(solution)/shard_map/all_to_all | solution.py:20
  86.8 0.1 convert_reduce_fusion.1
  86.9 0.1 copy.96
  87.0 0.1 add_convert_fusion
  87.1 0.7 copy.98
  (12 shorter events, 0.1 us)
Async XLA Ops:
  0.6 67.7 %copy-start = (bf16[176,2048]{1,0:T(8,128)(2,1)S(1)}, bf16[176,2048]{1,0:T(8,128)(2,1)}, u32[]{:S(2)}) copy-start(bf16[176,2048]{1,0:T(8,128)(2,1)} %param.33) | copy-start | bytes 2162692
  0.6 17.6 %copy-start.8 = (f32[8,4]{0,1:T(4,128)S(1)}, f32[8,4]{0,1:T(4,128)}, u32[]{:S(2)}) copy-start(f32[8,4]{0,1:T(4,128)} %param.27) | copy-start | bytes 388
  0.7 31.6 %copy-start.9 = (f32[4]{0:T(128)S(1)}, f32[4]{0:T(128)}, u32[]{:S(2)}) copy-start(f32[4]{0:T(128)} %param.24) | copy-start | bytes 52
  0.7 31.8 %copy-start.5 = (f32[8,4,128]{2,1,0:T(4,128)S(1)}, f32[8,4,128]{2,1,0:T(4,128)}, u32[]{:S(2)}) copy-start(f32[8,4,128]{2,1,0:T(4,128)} %param.26) | copy-start | bytes 49156
  8.4 27.8 %copy-start.7 = (f32[4,256]{1,0:T(4,128)S(1)}, f32[4,256]{1,0:T(4,128)}, u32[]{:S(2)}) copy-start(f32[4,256]{1,0:T(4,128)} %param.28) | copy-start | bytes 12292
  9.5 38.2 %copy-start.4 = (bf16[1024,128]{1,0:T(8,128)(2,1)S(1)}, bf16[1024,128]{1,0:T(8,128)(2,1)}, u32[]{:S(2)}) copy-start(bf16[1024,128]{1,0:T(8,128)(2,1)} %param.29) | copy-start | bytes 786436
  9.5 44.2 %copy-start.1 = (bf16[128,128]{1,0:T(8,128)(2,1)S(1)}, bf16[128,128]{1,0:T(8,128)(2,1)}, u32[]{:S(2)}) copy-start(bf16[128,128]{1,0:T(8,128)(2,1)} %param.17) | copy-start | bytes 98308
  9.5 22.3 %all-to-all-start = ((bf16[16,8,3081]{2,1,0:T(8,128)(2,1)}), bf16[16,8,3081]{2,1,0:T(8,128)(2,1)S(1)}, u32[]{:S(2)}, u32[]{:S(2)}) async-start(bf16[16,8,3081]{2,1,0:T(8,128)(2,1)} %concatenate.23), calls=%async_computation | async-start | bytes 1638400 | tf_op jit(solution)/shard_map/all_to_all | solution.py:20
  33.4 34.3 %copy-start.6 = (f32[2048]{0:T(1024)S(1)}, f32[2048]{0:T(1024)}, u32[]{:S(2)}) copy-start(f32[2048]{0:T(1024)} %param.30) | copy-start | bytes 24580
  33.4 34.6 %copy-start.2 = (bf16[2048,176]{0,1:T(8,128)(2,1)S(1)}, bf16[2048,176]{0,1:T(8,128)(2,1)}, u32[]{:S(2)}) copy-start(bf16[2048,176]{0,1:T(8,128)(2,1)} %param.31) | copy-start | bytes 2162692
  36.0 32.3 %copy-start.3 = (bf16[2048,176]{0,1:T(8,128)(2,1)S(1)}, bf16[2048,176]{0,1:T(8,128)(2,1)}, u32[]{:S(2)}) copy-start(bf16[2048,176]{0,1:T(8,128)(2,1)} %param.32) | copy-start | bytes 2162692
  70.0 16.8 %all-to-all-start.4 = ((bf16[32,128,64]{1,2,0:T(8,128)(2,1)}), bf16[32,128,64]{1,2,0:T(8,128)(2,1)S(1)}, u32[]{:S(2)}, u32[]{:S(2)}) async-start(bf16[32,128,64]{1,2,0:T(8,128)(2,1)} %bitcast.16), calls=%async_computation.4 | async-start | bytes 1048576 | tf_op jit(solution)/shard_map/all_to_all | solution.py:20
where the time goes:
time: 88.4 us; the launch traced here: 87.8 us
  blocking collectives  30.4 us (34%)
  waiting for transfers between devices  20.4 us (23%)
  starting transfers between devices  14 us (16%)
  matrix products  9.37 us (11%)
  other arithmetic  7.4 us (8%)
  local copies, waits for them, and re-layouts  5.34 us (6%)
  between operations  0.91 us (1%)
    all_to_all x3, blocking collectives, from_everyone(): lax.all_to_all(jnp.broadcast_to(value[None], (devices, *value.shape)), ax...  30.4 us
    all_to_all x2, waiting for transfers between devices, sum_at_owner(): lax.all_to_all(cut_along(value, dim, devices), axis, 0, 0, tiled=True)  20.4 us
    all_to_all x2, starting transfers between devices, sum_at_owner(): lax.all_to_all(cut_along(value, dim, devices), axis, 0, 0, tiled=True)  14 us
    add x1, other arithmetic, back_half(): forget_scale[..., None, None] * memory  3.97 us
    dot_general x1, matrix products, front_half(): carried = jnp.einsum('bhd,bhde->bhe', query_heads, memory)  2.64 us
  transfers between devices with their start and end apart: 2, of which 2 were waited for; matrix products, arithmetic and copies ran while one was open for 5% of the time, Pallas kernels for 0%

commit v1 on v0

v1 whole, which is shorter than its diff:
```python
import jax
import jax.numpy as jnp
from jax import lax
from jax.experimental import pallas as pl
from jax.experimental.pallas import tpu as pltpu
from jax.sharding import PartitionSpec as P

QK = 128
VD = 256
EPSILON = 1e-06
ROW = 4
KV = 16
SEQ = 8
HEADS = 4
MESH = pl.DeviceIdType.MESH
F32 = jnp.float32
BF16 = jnp.bfloat16

FAR = sorted(
    [(a, b) for a in range(ROW) for b in range(ROW) if (a, b) != (0, 0)],
    key=lambda o: -(min(o[0], ROW - o[0]) + min(o[1], ROW - o[1])),
)


def dot(a, b):
    return jnp.dot(a, b, preferred_element_type=F32)


def layer(
    tok_h, gain_h, wq_h, wk_h, wv_h, wo_h, wgates_h, bias_h, mem_h, nrm_h, stab_h, hgain_h, wout_h, mgain_h,
    wg_h, wu_h, wd_h,
    out_ref, nmem_ref, nnrm_ref, nstab_ref,
    tok, gain, wq, wk, wv, wo, wgates, bias, mem, nrm, stab, hgain, wout, mgain, wg, wu, wd,
    pwg, pwu, pwd, ext, a1_send, a1_recv, a2_send, a2_recv, carried, heads, half_send, half_recv, resid, rows,
    down_send, down_recv,
    in_sem, a_ssem, a_rsem, w_ssem, w_rsem, c_ssem, c_rsem, d_ssem, d_rsem, e_ssem, e_rsem, g_ssem, g_rsem,
):
    me = lax.axis_index("kv")
    tp = lax.axis_index("tp")
    z, y = me // ROW, me % ROW
    other = 1 - tp

    def chip(dz, dy):
        return ((z + dz) % ROW) * ROW + (y + dy) % ROW

    barrier = pltpu.get_barrier_semaphore()
    for dz, dy in FAR:
        for core in (tp, other):
            pl.semaphore_signal(
                barrier, inc=1, device_id={"kv": chip(dz, dy), "tp": core}, device_id_type=MESH
            )
    pl.semaphore_signal(barrier, inc=1, device_id={"tp": other}, device_id_type=MESH)

    loads = {}

    def load(name, src, dst):
        loads[name] = pltpu.make_async_copy(src, dst, in_sem.at[len(loads)])
        loads[name].start()

    load("tok", tok_h, tok)
    load("gain", gain_h, gain)
    load("wq", wq_h, wq)
    load("wk", wk_h, wk)
    load("wgates", wgates_h.at[pl.ds(pl.multiple_of(me * QK, QK), QK), :], wgates)
    load("wv", wv_h, wv)
    load("wo", wo_h, wo)
    load("mem", mem_h, mem)
    load("bias", bias_h, bias)
    load("nrm", nrm_h, nrm)
    load("stab", stab_h, stab)
    load("hgain", hgain_h, hgain)
    load("wout", wout_h, wout)
    load("mgain", mgain_h, mgain)
    load("wg", wg_h, wg)
    load("wu", wu_h, wu)
    load("wd", wd_h, wd)

    def ready(*names):
        for name in names:
            loads[name].wait()

    def send(src, dst, ssem, rsem, **device):
        pltpu.make_async_remote_copy(
            src_ref=src, dst_ref=dst, send_sem=ssem, recv_sem=rsem, device_id=device, device_id_type=MESH
        ).start()

    def wait_for(ref, sem):
        pltpu.make_async_copy(ref, ref, sem).wait()

    ready("tok", "gain")
    activations = tok[...].astype(F32)
    scaled = (activations * gain[...]).astype(BF16)
    square = jnp.sum(activations * activations, axis=1, keepdims=True)
    ext[...] = jnp.zeros_like(ext)
    ready("wq", "wk", "wgates")
    ext[:, 0:16] = dot(scaled, wgates[...])
    lane = lax.broadcasted_iota(jnp.int32, (128, 128), 1)
    extra = jnp.where(lane == 16, square, ext[...])

    def put(dst, at, value):
        dst[:, :, at : at + value.shape[1]] = value.reshape(KV, SEQ, value.shape[1]).astype(BF16)

    put(a1_send, 0, dot(scaled, wq[...]))
    put(a1_send, 512, dot(scaled, wk[...]))
    put(a1_send, 1024, extra)
    pl.semaphore_wait(barrier, 2 * KV - 1)
    for slot, (dz, dy) in enumerate(FAR):
        to = chip(dz, dy)
        send(a1_send.at[to], a1_recv.at[slot], a_ssem.at[0], a_rsem.at[0], kv=to)
    ready("wv", "wo")
    put(a2_send, 0, dot(scaled, wv[...]))
    put(a2_send, 1024, dot(scaled, wo[...]))
    for slot, (dz, dy) in enumerate(FAR):
        to = chip(dz, dy)
        send(a2_send.at[to], a2_recv.at[slot], a_ssem.at[1], a_rsem.at[1], kv=to)
    for at, (src, dst) in enumerate(((wg_h, pwg), (wu_h, pwu), (wd_h, pwd))):
        send(src, dst, w_ssem.at[at], w_rsem.at[at], tp=other)

    def total_of(own, others):
        total = own[me].astype(F32)
        for slot in range(KV - 1):
            total = total + others[slot].astype(F32)
        return total

    def by_head(value, width):
        return jnp.concatenate([value[:, h * width : (h + 1) * width] for h in range(HEADS)], axis=0)

    wait_for(a1_recv, a_rsem.at[0])
    first = total_of(a1_send, a1_recv)
    inverse = lax.rsqrt(first[:, 1040:1041] * (1.0 / (KV * QK)) + EPSILON)
    query = (first[:, 0:512] * inverse).astype(BF16).astype(F32)
    key = (first[:, 512:1024] * (inverse * QK ** (-0.5))).astype(BF16).astype(F32)
    gate_pre = first[:, 1024:1152] * inverse
    low = tp == 0
    input_pre = jnp.where(low, gate_pre[:, 0:4], gate_pre[:, 4:8])
    forget_pre = jnp.where(low, gate_pre[:, 8:12], gate_pre[:, 12:16])
    ready("bias", "nrm", "stab", "hgain")
    raw = forget_pre + bias[...]
    log_forget = jnp.minimum(raw, 0.0) - jnp.log1p(jnp.exp(-jnp.abs(raw)))
    shifted = log_forget + stab[...]
    new_stab = jnp.maximum(shifted, input_pre)
    nstab_ref[...] = new_stab
    forget_scale = by_head(jnp.exp(shifted - new_stab), 1)
    input_scale = by_head(jnp.exp(input_pre - new_stab), 1)
    query_heads = by_head(query, QK)
    key_heads = by_head(key, QK)
    old_normalizer = jnp.concatenate([nrm[:, h, :] for h in range(HEADS)], axis=0)
    new_normalizer = forget_scale * old_normalizer + input_scale * key_heads
    for h in range(HEADS):
        nnrm_ref[:, h, :] = new_normalizer[h * SEQ : (h + 1) * SEQ]
    denominator = jnp.sum(query_heads * new_normalizer, axis=1, keepdims=True)
    query_key = jnp.sum(query_heads * key_heads, axis=1, keepdims=True)
    query_cols = jnp.transpose(query_heads).astype(BF16)
    key_cols = jnp.transpose(key_heads).astype(BF16)
    pair_row = lax.broadcasted_iota(jnp.int32, (HEADS * SEQ, QK), 0)
    ready("mem")
    for pair in range(HEADS * SEQ):
        h, s = pair // SEQ, pair % SEQ
        spread = dot(query_cols, jnp.where(pair_row == pair, 1.0, 0.0).astype(BF16))
        old = mem[s, h]
        low_half = jnp.sum(old[:, 0:128] * spread, axis=0, keepdims=True)
        high_half = jnp.sum(old[:, 128:256] * spread, axis=0, keepdims=True)
        carried[pair : pair + 1, 0:128] = low_half
        carried[pair : pair + 1, 128:256] = high_half

    wait_for(a2_recv, a_rsem.at[1])
    second = total_of(a2_send, a2_recv) * inverse
    value_heads = by_head(second[:, 0:1024].astype(BF16).astype(F32), VD)
    outgate = by_head(second[:, 1024:2048].astype(BF16).astype(F32), VD)
    numerator = forget_scale * carried[...] + (input_scale * query_key) * value_heads
    head_out = numerator / jnp.maximum(jnp.abs(denominator), 1.0)
    gain_rows = jnp.concatenate(
        [jnp.broadcast_to(hgain[h : h + 1, :], (SEQ, VD)) for h in range(HEADS)], axis=0
    )
    normed = (
        head_out * lax.rsqrt(jnp.mean(head_out * head_out, axis=1, keepdims=True) + EPSILON) * gain_rows
    )
    mixed = normed * jax.nn.sigmoid(outgate)
    heads[me] = jnp.concatenate(
        [mixed[h * SEQ : (h + 1) * SEQ] for h in range(HEADS)], axis=1
    ).astype(BF16)

    for dz, dy in FAR:
        send(heads.at[me], heads.at[me], c_ssem, c_rsem, kv=chip(dz, dy))
    value_row = lax.broadcasted_iota(jnp.int32, (HEADS * SEQ, VD), 0)
    for pair in range(HEADS * SEQ):
        h, s = pair // SEQ, pair % SEQ
        outer = dot(key_cols, jnp.where(value_row == pair, value_heads, 0.0).astype(BF16))
        nmem_ref[s, h] = (
            forget_scale[pair : pair + 1, :] * mem[s, h] + input_scale[pair : pair + 1, :] * outer
        )
    ready("wout", "mgain")
    wait_for(heads.at[0:15], c_rsem)
    gathered = heads[...].astype(F32).reshape(KV * SEQ, HEADS * VD).astype(BF16)

    half_send[...] = dot(gathered, wout[...]).astype(BF16)
    send(half_send, half_recv, d_ssem, d_rsem, tp=other)
    wait_for(half_recv, d_rsem)
    branch = half_send[...].astype(F32) + half_recv[...].astype(F32)
    residual = (tok[...].astype(F32) + branch).astype(BF16)
    resid[...] = residual.astype(F32)
    rows[me] = jnp.where(low, resid[0:64, :], resid[64:128, :]).astype(BF16)

    for dz, dy in FAR:
        send(rows.at[me], rows.at[me], e_ssem, e_rsem, kv=chip(dz, dy))
    ready("wg", "wu", "wd")
    wait_for(pwg, w_rsem.at[0])
    wait_for(pwu, w_rsem.at[1])
    wait_for(pwd, w_rsem.at[2])
    wait_for(rows.at[0:15], e_rsem)
    whole = jnp.concatenate([rows[j].astype(F32) for j in range(KV)], axis=1)
    inverse_two = lax.rsqrt(jnp.mean(whole * whole, axis=1, keepdims=True) + EPSILON)
    mlp_in = (whole * inverse_two * mgain[...]).astype(BF16)

    def hidden_of(gate_w, up_w):
        return (jax.nn.silu(dot(mlp_in, gate_w[...])) * dot(mlp_in, up_w[...])).astype(BF16)

    hidden_own = hidden_of(wg, wu)
    hidden_other = hidden_of(pwg, pwu)

    lane_two = lax.broadcasted_iota(jnp.int32, (32, 128), 1)
    slot = me * 2 + tp
    for dz in (2, 1, 3, 0):
        cols = pl.ds(pl.multiple_of(((z + dz) % ROW) * 512, 512), 512)
        part = dot(hidden_own, wd[:, cols]) + dot(hidden_other, pwd[:, cols])
        for at in range(ROW):
            top = part[0:32, at * 128 : (at + 1) * 128]
            bottom = part[32:64, at * 128 : (at + 1) * 128]
            down_send[dz, at, 0] = jnp.where(lane_two < 64, top, pltpu.roll(bottom, 64, 1)).astype(BF16)
            down_send[dz, at, 1] = jnp.where(lane_two < 64, pltpu.roll(top, 64, 1), bottom).astype(BF16)
        for dy in (2, 1, 3, 0):
            column = (y + dy) % ROW
            for core in (tp, other):
                if (dz, dy) != (0, 0) or core is other:
                    send(
                        down_send.at[dz, column, core], down_recv.at[slot], g_ssem, g_rsem,
                        kv=chip(dz, dy), tp=core,
                    )
    down_recv[slot] = down_send[0, y, tp]
    wait_for(down_recv.at[0:31], g_rsem)
    pieces = []
    for core in range(2):
        total = down_recv[core].astype(F32)
        for j in range(1, KV):
            total = total + down_recv[2 * j + core].astype(F32)
        pieces += [total[:, 0:64], total[:, 64:128]]
    summed = jnp.concatenate(pieces, axis=0)
    own = jnp.where(low, resid[:, 0:64], resid[:, 64:128])
    out_ref[...] = (summed + own).astype(BF16)

    wait_for(a1_recv, a_ssem.at[0])
    wait_for(a2_recv, a_ssem.at[1])
    wait_for(pwg, w_ssem.at[0])
    wait_for(pwu, w_ssem.at[1])
    wait_for(pwd, w_ssem.at[2])
    wait_for(heads.at[0:15], c_ssem)
    wait_for(half_send, d_ssem)
    wait_for(rows.at[0:15], e_ssem)
    wait_for(down_recv.at[0:31], g_ssem)


def body(tokens, mix_gain, w_query, w_key, w_value, w_outgate, w_gates, forget_bias, memory, normalizer, stabilizer,
         head_gain, w_out, mlp_gain, w_gate, w_up, w_down):
    args = (
        tokens, mix_gain.reshape(1, -1), w_query, w_key, w_value, w_outgate, w_gates, forget_bias.reshape(1, -1),
        memory, normalizer, stabilizer, head_gain, w_out, mlp_gain.reshape(1, -1), w_gate, w_up, w_down,
    )
    copies = [pltpu.VMEM(a.shape, a.dtype) for a in args]
    copies[6] = pltpu.VMEM((QK, 16), BF16)
    dma = pltpu.SemaphoreType.DMA
    return pl.pallas_call(
        layer,
        name="layer",
        out_shape=(
            jax.ShapeDtypeStruct((128, 64), BF16),
            jax.ShapeDtypeStruct(memory.shape, F32),
            jax.ShapeDtypeStruct(normalizer.shape, F32),
            jax.ShapeDtypeStruct(stabilizer.shape, F32),
        ),
        in_specs=[pl.BlockSpec(memory_space=pl.ANY)] * len(args),
        out_specs=[pl.BlockSpec(memory_space=pltpu.VMEM)] * 4,
        scratch_shapes=copies + [
            pltpu.VMEM(w_gate.shape, BF16),
            pltpu.VMEM(w_up.shape, BF16),
            pltpu.VMEM(w_down.shape, BF16),
            pltpu.VMEM((128, 128), F32),
            pltpu.VMEM((KV, SEQ, 1152), BF16),
            pltpu.VMEM((KV - 1, SEQ, 1152), BF16),
            pltpu.VMEM((KV, SEQ, 2048), BF16),
            pltpu.VMEM((KV - 1, SEQ, 2048), BF16),
            pltpu.VMEM((HEADS * SEQ, VD), F32),
            pltpu.VMEM((KV, SEQ, HEADS * VD), BF16),
            pltpu.VMEM((128, 128), BF16),
            pltpu.VMEM((128, 128), BF16),
            pltpu.VMEM((128, 128), F32),
            pltpu.VMEM((KV, 64, 128), BF16),
            pltpu.VMEM((ROW, ROW, 2, 32, 128), BF16),
            pltpu.VMEM((2 * KV, 32, 128), BF16),
            dma((len(args),)), dma((2,)), dma((2,)), dma((3,)), dma((3,)),
            dma, dma, dma, dma, dma, dma, dma, dma,
        ],
        compiler_params=pltpu.CompilerParams(
            collective_id=0, has_side_effects=True, vmem_limit_bytes=48 * 1024 * 1024
        ),
    )(*args)


def solution(mesh):
    in_specs = (
        P("dp", "kv"), P("kv"), P("kv", "tp"), P("kv", "tp"), P("kv", "tp"), P("kv", "tp"), P(), P("tp"),
        P(("dp", "kv"), "tp", None, None), P(("dp", "kv"), "tp", None), P(("dp", "kv"), "tp"), P("tp", None),
        P("tp", "kv"), P(), P(None, ("kv", "tp")), P(None, ("kv", "tp")), P(("kv", "tp"), None),
    )
    out_specs = (
        P("dp", ("kv", "tp")), P(("dp", "kv"), "tp", None, None), P(("dp", "kv"), "tp", None), P(("dp", "kv"), "tp"),
    )
    return jax.shard_map(body, mesh=mesh, in_specs=in_specs, out_specs=out_specs, check_vma=False)
```

time: 88.4 us -> 60.7 us (0.69)
  Pallas kernels: 0 us -> 40.1 us
  blocking collectives: 30.4 us -> 0 us
  waiting for transfers between devices: 20.4 us -> 0 us
  starting transfers between devices: 14 us -> 0 us
  local copies, waits for them, and re-layouts: 5.34 us -> 19.3 us
  matrix products: 9.37 us -> 0 us
  other arithmetic: 7.4 us -> 0 us
    pallas_call x0 -> x1, Pallas kernels: none -> 40.1 us  [body(): pl.pallas_call(layer, name='layer', out_shape=(jax.ShapeDtypeStruct((128,...]
    all_to_all x3 -> x0, blocking collectives: 30.4 us -> none  [from_everyone(): lax.all_to_all(jnp.broadcast_to(value[None], (devices, *value.shape)), ax...]
    all_to_all x2 -> x0, waiting for transfers between devices: 20.4 us -> none  [sum_at_owner(): lax.all_to_all(cut_along(value, dim, devices), axis, 0, 0, tiled=True)]
    unnamed x23 -> x30, local copies, waits for them, and re-layouts: 1.48 us -> 18 us
    all_to_all x2 -> x0, starting transfers between devices: 14 us -> none  [sum_at_owner(): lax.all_to_all(cut_along(value, dim, devices), axis, 0, 0, tiled=True)]
    dot_general x9 -> x0, matrix products: 9.37 us -> none  [the longest x1 2.64 us: front_half(): carried = jnp.einsum('bhd,bhde->bhe', query_heads, memory)]
    add x1 -> x0, other arithmetic: 3.97 us -> none  [back_half(): forget_scale[..., None, None] * memory]
    reduce_sum x7 -> x0, other arithmetic: 2.28 us -> none  [the longest x1 0.92 us: body(): square_part = jnp.sum(activations * activations, axis=1, keepdims=True)]
  transfers between devices with their start and end apart: 2 -> 0, of which waited for: 2 -> 0; matrix products, arithmetic and copies ran while one was open for 5% -> 0% of each run, Pallas kernels for 0% -> 0%
where the time goes in v1:
time: 60.7 us; the launch traced here: 60.2 us
  Pallas kernels  40.1 us (66%)
  local copies, waits for them, and re-layouts  19.3 us (32%)
  between operations  0.71 us (1%)
    pallas_call x1, Pallas kernels, body(): pl.pallas_call(layer, name='layer', out_shape=(jax.ShapeDtypeStruct((128,...  40.1 us
    unnamed x30, local copies, waits for them, and re-layouts  18 us
    pallas_call x2, local copies, waits for them, and re-layouts, body(): pl.pallas_call(layer, name='layer', out_shape=(jax.ShapeDtypeStruct((128,...  1.35 us

profile of v1, /device:TPU:1, one launch (start us, length us, event | category | flops | bytes accessed | tf_op | source)
XLA Modules:
  0.0 60.2 jit_solution(5663882901195844867)
XLA Ops:
  0.6 0.0 copy-start
  0.6 0.0 copy-start.4
  0.7 0.8 %copy.22.stab_h = f32[8,4]{1,0:T(8,128)S(1)} copy(f32[8,4]{0,1:T(4,128)} %param.27) | data formatting | bytes 256 | tf_op args[10]
  1.5 1.1 %copy.21.wgates_h = bf16[2048,16]{1,0:T(8,128)(2,1)S(1)} copy(bf16[2048,16]{0,1:T(8,128)(2,1)} %param.23) | data formatting | bytes 131072 | tf_op args[6]
  2.6 1.4 %copy.23.wg_h = bf16[2048,176]{1,0:T(8,128)(2,1)S(1)} copy(bf16[2048,176]{0,1:T(8,128)(2,1)} %param.31) | data formatting | bytes 1441792 | tf_op args[14]
  4.0 1.4 %copy.24.wu_h = bf16[2048,176]{1,0:T(8,128)(2,1)S(1)} copy(bf16[2048,176]{0,1:T(8,128)(2,1)} %param.32) | data formatting | bytes 1441792 | tf_op args[15]
  5.5 0.0 copy-done
  5.5 0.0 copy-done.4
  5.5 0.0 copy-start.1
  5.5 0.9 %copy-done.1 = bf16[128,1024]{1,0:T(8,128)(2,1)S(1)} copy-done((bf16[128,1024]{1,0:T(8,128)(2,1)S(1)}, bf16[128,1024]{1,0:T(8,128)(2,1)}, u32[]{:S(2)}) %copy-start.1) | copy-done | bytes 262168
  6.4 0.0 copy-start.2
  6.4 0.9 %copy-done.2 = bf16[128,1024]{1,0:T(8,128)(2,1)S(1)} copy-done((bf16[128,1024]{1,0:T(8,128)(2,1)S(1)}, bf16[128,1024]{1,0:T(8,128)(2,1)}, u32[]{:S(2)}) %copy-start.2) | copy-done | bytes 262168
  7.4 0.0 copy-start.3
  7.4 0.9 %copy-done.3 = bf16[1024,128]{1,0:T(8,128)(2,1)S(1)} copy-done((bf16[1024,128]{1,0:T(8,128)(2,1)S(1)}, bf16[1024,128]{1,0:T(8,128)(2,1)}, u32[]{:S(2)}) %copy-start.3) | copy-done | bytes 262168
  8.3 0.0 copy-start.5
  8.3 0.9 %copy-done.5 = bf16[128,512]{1,0:T(8,128)(2,1)S(1)} copy-done((bf16[128,512]{1,0:T(8,128)(2,1)S(1)}, bf16[128,512]{1,0:T(8,128)(2,1)}, u32[]{:S(2)}) %copy-start.5) | copy-done | bytes 131096
  9.2 0.0 copy-start.6
  9.2 0.8 %copy-done.6 = bf16[128,128]{1,0:T(8,128)(2,1)S(1)} copy-done((bf16[128,128]{1,0:T(8,128)(2,1)S(1)}, bf16[128,128]{1,0:T(8,128)(2,1)}, u32[]{:S(2)}) %copy-start.6) | copy-done | bytes 32792
  10.0 0.0 copy-start.7
  10.0 0.7 %copy-done.7 = f32[8,4,128]{2,1,0:T(4,128)S(1)} copy-done((f32[8,4,128]{2,1,0:T(4,128)S(1)}, f32[8,4,128]{2,1,0:T(4,128)}, u32[]{:S(2)}) %copy-start.7) | copy-done | bytes 16408
  10.7 0.0 copy-start.8
  10.7 0.7 %copy-done.8 = f32[2048]{0:T(1024)S(1)} copy-done((f32[2048]{0:T(1024)S(1)}, f32[2048]{0:T(1024)}, u32[]{:S(2)}) %copy-start.8) | copy-done | bytes 8216
  11.4 0.0 copy-start.9
  11.4 0.7 %copy-done.9 = f32[4,256]{1,0:T(4,128)S(1)} copy-done((f32[4,256]{1,0:T(4,128)S(1)}, f32[4,256]{1,0:T(4,128)}, u32[]{:S(2)}) %copy-start.9) | copy-done | bytes 4120
  12.1 0.0 copy-start.10
  12.1 0.7 %copy-done.10 = f32[128]{0:T(128)S(1)} copy-done((f32[128]{0:T(128)S(1)}, f32[128]{0:T(128)}, u32[]{:S(2)}) %copy-start.10) | copy-done | bytes 536
  12.8 0.0 copy-start.11
  12.8 0.7 %copy-done.11 = f32[4]{0:T(128)S(1)} copy-done((f32[4]{0:T(128)S(1)}, f32[4]{0:T(128)}, u32[]{:S(2)}) %copy-start.11) | copy-done | bytes 40
  13.4 40.1 %layer.1 = (bf16[128,64]{1,0:T(8,128)(2,1)S(1)}, f32[8,4,128,256]{3,2,1,0:T(8,128)}, f32[8,4,128]{2,1,0:T(4,128)S(1)}, f32[8,4]{1,0:T(8,128)S(1)}) custom-call(bf16[128,128]{1,0:T(8,128)(2,1)S(1)} %copy-done.6, f32[1,128]{1,0:T(1,128)S(1)} %bitcast.4, bf16[128,512]{1,0:T(8,128)(2,1)S(1)} %copy-done.4, bf16[128,512]{1,0:T(8,128)(2,1)S(1)} %copy-done.5, ...), custom_call_target="tpu_custom_call" | custom-call | tf_op jit(solution)/shard_map/layer/pallas_call | solution.py:271
  53.6 0.7 %copy.25 = bf16[128,64]{0,1:T(8,128)(2,1)} copy(bf16[128,64]{1,0:T(8,128)(2,1)S(1)} %get-tuple-element.4) | data formatting | bytes 32768 | tf_op jit(solution)/shard_map/layer/pallas_call | solution.py:271
  54.3 0.7 %copy.26 = f32[8,4]{0,1:T(4,128)} copy(f32[8,4]{1,0:T(8,128)S(1)} %get-tuple-element.7) | data formatting | bytes 256 | tf_op jit(solution)/shard_map/layer/pallas_call | solution.py:271
  54.9 4.7 %copy.29 = f32[8,4,128,256]{3,2,1,0:T(8,128)} copy(f32[8,4,128,256]{3,2,1,0:T(8,128)} %get-tuple-element.13) | data formatting | bytes 8388608
  59.6 0.6 %copy.30 = f32[8,4,128]{2,1,0:T(4,128)} copy(f32[8,4,128]{2,1,0:T(4,128)S(1)} %get-tuple-element.14) | data formatting | bytes 32768
Async XLA Ops:
  0.6 4.8 %copy-start = (bf16[176,2048]{1,0:T(8,128)(2,1)S(1)}, bf16[176,2048]{1,0:T(8,128)(2,1)}, u32[]{:S(2)}) copy-start(bf16[176,2048]{1,0:T(8,128)(2,1)} %wd_h.1) | copy-start | bytes 2162692
  0.6 4.8 %copy-start.4 = (bf16[128,512]{1,0:T(8,128)(2,1)S(1)}, bf16[128,512]{1,0:T(8,128)(2,1)}, u32[]{:S(2)}) copy-start(bf16[128,512]{1,0:T(8,128)(2,1)} %wq_h.1) | copy-start | bytes 393220
  5.5 1.0 %copy-start.1 = (bf16[128,1024]{1,0:T(8,128)(2,1)S(1)}, bf16[128,1024]{1,0:T(8,128)(2,1)}, u32[]{:S(2)}) copy-start(bf16[128,1024]{1,0:T(8,128)(2,1)} %wv_h.1) | copy-start | bytes 786436
  6.4 0.9 %copy-start.2 = (bf16[128,1024]{1,0:T(8,128)(2,1)S(1)}, bf16[128,1024]{1,0:T(8,128)(2,1)}, u32[]{:S(2)}) copy-start(bf16[128,1024]{1,0:T(8,128)(2,1)} %wo_h.1) | copy-start | bytes 786436
  7.4 0.9 %copy-start.3 = (bf16[1024,128]{1,0:T(8,128)(2,1)S(1)}, bf16[1024,128]{1,0:T(8,128)(2,1)}, u32[]{:S(2)}) copy-start(bf16[1024,128]{1,0:T(8,128)(2,1)} %wout_h.1) | copy-start | bytes 786436
  8.3 0.9 %copy-start.5 = (bf16[128,512]{1,0:T(8,128)(2,1)S(1)}, bf16[128,512]{1,0:T(8,128)(2,1)}, u32[]{:S(2)}) copy-start(bf16[128,512]{1,0:T(8,128)(2,1)} %wk_h.1) | copy-start | bytes 393220
  9.2 0.8 %copy-start.6 = (bf16[128,128]{1,0:T(8,128)(2,1)S(1)}, bf16[128,128]{1,0:T(8,128)(2,1)}, u32[]{:S(2)}) copy-start(bf16[128,128]{1,0:T(8,128)(2,1)} %tok_h.1) | copy-start | bytes 98308
  10.0 0.7 %copy-start.7 = (f32[8,4,128]{2,1,0:T(4,128)S(1)}, f32[8,4,128]{2,1,0:T(4,128)}, u32[]{:S(2)}) copy-start(f32[8,4,128]{2,1,0:T(4,128)} %nrm_h.1) | copy-start | bytes 49156
  10.7 0.7 %copy-start.8 = (f32[2048]{0:T(1024)S(1)}, f32[2048]{0:T(1024)}, u32[]{:S(2)}) copy-start(f32[2048]{0:T(1024)} %param.30) | copy-start | bytes 24580
  11.4 0.7 %copy-start.9 = (f32[4,256]{1,0:T(4,128)S(1)}, f32[4,256]{1,0:T(4,128)}, u32[]{:S(2)}) copy-start(f32[4,256]{1,0:T(4,128)} %hgain_h.1) | copy-start | bytes 12292
  12.1 0.7 %copy-start.10 = (f32[128]{0:T(128)S(1)}, f32[128]{0:T(128)}, u32[]{:S(2)}) copy-start(f32[128]{0:T(128)} %param.18) | copy-start | bytes 1540
  12.8 0.7 %copy-start.11 = (f32[4]{0:T(128)S(1)}, f32[4]{0:T(128)}, u32[]{:S(2)}) copy-start(f32[4]{0:T(128)} %param.24) | copy-start | bytes 52

commit v2 on v1

--- a/solution.py
+++ b/solution.py
@@ -24,6 +24,10 @@
 
 def dot(a, b):
     return jnp.dot(a, b, preferred_element_type=F32)
+
+
+def dot_rows(a, b):
+    return lax.dot_general(a, b, (((1,), (1,)), ((), ())), preferred_element_type=F32)
 
 
 def layer(
@@ -61,7 +65,7 @@
     load("gain", gain_h, gain)
     load("wq", wq_h, wq)
     load("wk", wk_h, wk)
-    load("wgates", wgates_h.at[pl.ds(pl.multiple_of(me * QK, QK), QK), :], wgates)
+    load("wgates", wgates_h.at[:, pl.ds(pl.multiple_of(me * QK, QK), QK)], wgates)
     load("wv", wv_h, wv)
     load("wo", wo_h, wo)
     load("mem", mem_h, mem)
@@ -93,7 +97,7 @@
     square = jnp.sum(activations * activations, axis=1, keepdims=True)
     ext[...] = jnp.zeros_like(ext)
     ready("wq", "wk", "wgates")
-    ext[:, 0:16] = dot(scaled, wgates[...])
+    ext[:, 0:16] = dot_rows(scaled, wgates[...])
     lane = lax.broadcasted_iota(jnp.int32, (128, 128), 1)
     extra = jnp.where(lane == 16, square, ext[...])
 
@@ -137,9 +141,20 @@
     ready("bias", "nrm", "stab", "hgain")
     raw = forget_pre + bias[...]
     log_forget = jnp.minimum(raw, 0.0) - jnp.log1p(jnp.exp(-jnp.abs(raw)))
-    shifted = log_forget + stab[...]
+    diagonal = lax.broadcasted_iota(jnp.int32, (SEQ, SEQ), 0) == lax.broadcasted_iota(jnp.int32, (SEQ, SEQ), 1)
+    old_stab = jnp.concatenate(
+        [
+            jnp.sum(jnp.where(diagonal, stab[h : h + 1, :], 0.0), axis=1, keepdims=True)
+            for h in range(HEADS)
+        ],
+        axis=1,
+    )
+    shifted = log_forget + old_stab
     new_stab = jnp.maximum(shifted, input_pre)
-    nstab_ref[...] = new_stab
+    for h in range(HEADS):
+        nstab_ref[h : h + 1, :] = jnp.sum(
+            jnp.where(diagonal, new_stab[:, h : h + 1], 0.0), axis=0, keepdims=True
+        )
     forget_scale = by_head(jnp.exp(shifted - new_stab), 1)
     input_scale = by_head(jnp.exp(input_pre - new_stab), 1)
     query_heads = by_head(query, QK)
@@ -213,7 +228,7 @@
     mlp_in = (whole * inverse_two * mgain[...]).astype(BF16)
 
     def hidden_of(gate_w, up_w):
-        return (jax.nn.silu(dot(mlp_in, gate_w[...])) * dot(mlp_in, up_w[...])).astype(BF16)
+        return (jax.nn.silu(dot_rows(mlp_in, gate_w[...])) * dot_rows(mlp_in, up_w[...])).astype(BF16)
 
     hidden_own = hidden_of(wg, wu)
     hidden_other = hidden_of(pwg, pwu)
@@ -243,10 +258,11 @@
         total = down_recv[core].astype(F32)
         for j in range(1, KV):
             total = total + down_recv[2 * j + core].astype(F32)
-        pieces += [total[:, 0:64], total[:, 64:128]]
-    summed = jnp.concatenate(pieces, axis=0)
-    own = jnp.where(low, resid[:, 0:64], resid[:, 64:128])
-    out_ref[...] = (summed + own).astype(BF16)
+        pieces += [total, pltpu.roll(total, 64, 1)]
+    own = resid[...]
+    own = jnp.where(low, own, pltpu.roll(own, 64, 1))
+    summed = jnp.concatenate(pieces, axis=0) + own
+    out_ref[...] = jnp.transpose(summed)[0:64, :].astype(BF16)
 
     wait_for(a1_recv, a_ssem.at[0])
     wait_for(a2_recv, a_ssem.at[1])
@@ -259,29 +275,40 @@
     wait_for(down_recv.at[0:31], g_ssem)
 
 
+def finish(out, nmem, nnrm, nstab, out_h, nmem_h, nnrm_h, nstab_h, sem):
+    copies = [(nmem.at[j], nmem_h.at[j]) for j in range(SEQ)]
+    copies += [(nnrm, nnrm_h), (nstab, nstab_h), (out, out_h)]
+    copies = [pltpu.make_async_copy(src, dst, sem.at[at]) for at, (src, dst) in enumerate(copies)]
+    for copy in copies:
+        copy.start()
+    for copy in copies:
+        copy.wait()
+
+
 def body(tokens, mix_gain, w_query, w_key, w_value, w_outgate, w_gates, forget_bias, memory, normalizer, stabilizer,
          head_gain, w_out, mlp_gain, w_gate, w_up, w_down):
     args = (
-        tokens, mix_gain.reshape(1, -1), w_query, w_key, w_value, w_outgate, w_gates, forget_bias.reshape(1, -1),
-        memory, normalizer, stabilizer, head_gain, w_out, mlp_gain.reshape(1, -1), w_gate, w_up, w_down,
+        tokens, mix_gain.reshape(1, -1), w_query, w_key, w_value, w_outgate, w_gates.T, forget_bias.reshape(1, -1),
+        memory, normalizer, stabilizer.T, head_gain, w_out, mlp_gain.reshape(1, -1), w_gate.T, w_up.T, w_down,
     )
     copies = [pltpu.VMEM(a.shape, a.dtype) for a in args]
-    copies[6] = pltpu.VMEM((QK, 16), BF16)
+    copies[6] = pltpu.VMEM((16, QK), BF16)
     dma = pltpu.SemaphoreType.DMA
-    return pl.pallas_call(
+    outs = (
+        jax.ShapeDtypeStruct((64, 128), BF16),
+        jax.ShapeDtypeStruct(memory.shape, F32),
+        jax.ShapeDtypeStruct(normalizer.shape, F32),
+        jax.ShapeDtypeStruct((HEADS, SEQ), F32),
+    )
+    results = pl.pallas_call(
         layer,
         name="layer",
-        out_shape=(
-            jax.ShapeDtypeStruct((128, 64), BF16),
-            jax.ShapeDtypeStruct(memory.shape, F32),
-            jax.ShapeDtypeStruct(normalizer.shape, F32),
-            jax.ShapeDtypeStruct(stabilizer.shape, F32),
-        ),
-        in_specs=[pl.BlockSpec(memory_space=pl.ANY)] * len(args),
+        out_shape=tuple(pltpu.VMEM(o.shape, o.dtype) for o in outs),
+        in_specs=[pl.BlockSpec(memory_space=pltpu.HBM)] * len(args),
         out_specs=[pl.BlockSpec(memory_space=pltpu.VMEM)] * 4,
         scratch_shapes=copies + [
-            pltpu.VMEM(w_gate.shape, BF16),
-            pltpu.VMEM(w_up.shape, BF16),
+            pltpu.VMEM(w_gate.shape[::-1], BF16),
+            pltpu.VMEM(w_up.shape[::-1], BF16),
             pltpu.VMEM(w_down.shape, BF16),
             pltpu.VMEM((128, 128), F32),
             pltpu.VMEM((KV, SEQ, 1152), BF16),
@@ -300,9 +327,19 @@
             dma, dma, dma, dma, dma, dma, dma, dma,
         ],
         compiler_params=pltpu.CompilerParams(
-            collective_id=0, has_side_effects=True, vmem_limit_bytes=48 * 1024 * 1024
+            collective_id=0, has_side_effects=True, vmem_limit_bytes=40 * 1024 * 1024
         ),
-    )(*args)
+    )(*(pltpu.with_memory_space_constraint(a, pltpu.HBM) for a in args))
+    out, new_memory, new_normalizer, new_stabilizer = pl.pallas_call(
+        finish,
+        name="finish",
+        out_shape=outs,
+        in_specs=[pl.BlockSpec(memory_space=pltpu.VMEM)] * 4,
+        out_specs=[pl.BlockSpec(memory_space=pltpu.HBM)] * 4,
+        scratch_shapes=[dma((SEQ + 3,))],
+        compiler_params=pltpu.CompilerParams(vmem_limit_bytes=8 * 1024 * 1024),
+    )(*results)
+    return out.T, new_memory, new_normalizer, new_stabilizer.T
 
 
 def solution(mesh):

time: 60.7 us -> 41.5 us (0.68)
  local copies, waits for them, and re-layouts: 19.3 us -> 0 us
    unnamed x30 -> x0, local copies, waits for them, and re-layouts: 18 us -> none
    pallas_call x2 -> x0, local copies, waits for them, and re-layouts: 1.35 us -> none  [body(): pl.pallas_call(layer, name='layer', out_shape=(jax.ShapeDtypeStruct((128,...]
    pallas_call x1 -> x2, Pallas kernels: 40.1 us -> 40.7 us  [the longest x1 38.6 us: body(): pl.pallas_call(layer, name='layer', out_shape=tuple((pltpu.VMEM(o.shape,...]
where the time goes in v2:
time: 41.5 us; the launch traced here: 41.4 us
  Pallas kernels  40.7 us (98%)
  between operations  0.65 us (2%)
    pallas_call x1, Pallas kernels, body(): pl.pallas_call(layer, name='layer', out_shape=tuple((pltpu.VMEM(o.shape,...  38.6 us
    pallas_call x1, Pallas kernels, body(): pl.pallas_call(finish, name='finish', out_shape=outs, in_specs=[pl.BlockS...  2.11 us

profile of v2, /device:TPU:1, one launch (start us, length us, event | category | flops | bytes accessed | tf_op | source)
XLA Modules:
  0.0 41.4 jit_solution(5737824780798610085)
XLA Ops:
  0.6 38.6 %layer.1 = (bf16[64,128]{1,0:T(8,128)(2,1)S(1)}, f32[8,4,128,256]{3,2,1,0:T(8,128)S(1)}, f32[8,4,128]{2,1,0:T(4,128)S(1)}, f32[4,8]{1,0:T(4,128)S(1)}) custom-call(bf16[128,128]{1,0:T(8,128)(2,1)} %tok_h.1, f32[1,128]{1,0:T(1,128)} %bitcast.14, bf16[128,512]{1,0:T(8,128)(2,1)} %wq_h.1, bf16[128,512]{1,0:T(8,128)(2,1)} %wk_h.1, bf16[128,1024]{1,0:T(8,128)(2,1)} %wv_h.1, ...), custom_call_target="tpu_custom_call" | custom-call | tf_op jit(solution)/shard_map/layer/pallas_call | solution.py:303
  39.2 2.1 %finish.1 = (bf16[64,128]{1,0:T(8,128)(2,1)}, f32[8,4,128,256]{3,2,1,0:T(8,128)}, f32[8,4,128]{2,1,0:T(4,128)}, f32[4,8]{1,0:T(4,128)}) custom-call(bf16[64,128]{1,0:T(8,128)(2,1)S(1)} %get-tuple-element.12.out, f32[8,4,128,256]{3,2,1,0:T(8,128)S(1)} %get-tuple-element.13.nmem, f32[8,4,128]{2,1,0:T(4,128)S(1)} %get-tuple-element.14.nnrm, ...), custom_call_target="tpu_custom_call" | custom-call | tf_op jit(solution)/shard_map/finish/pallas_call | solution.py:333

commit v3 on v2

--- a/solution.py
+++ b/solution.py
@@ -35,7 +35,7 @@
     wg_h, wu_h, wd_h,
     out_ref, nmem_ref, nnrm_ref, nstab_ref,
     tok, gain, wq, wk, wv, wo, wgates, bias, mem, nrm, stab, hgain, wout, mgain, wg, wu, wd,
-    pwg, pwu, pwd, ext, a1_send, a1_recv, a2_send, a2_recv, carried, heads, half_send, half_recv, resid, rows,
+    pwg, pwu, pwd, pwout, ext, a1_send, a1_recv, a2_send, a2_recv, carried, mixed_ref, heads, resid, rows,
     down_send, down_recv,
     in_sem, a_ssem, a_rsem, w_ssem, w_rsem, c_ssem, c_rsem, d_ssem, d_rsem, e_ssem, e_rsem, g_ssem, g_rsem,
 ):
@@ -117,7 +117,7 @@
     for slot, (dz, dy) in enumerate(FAR):
         to = chip(dz, dy)
         send(a2_send.at[to], a2_recv.at[slot], a_ssem.at[1], a_rsem.at[1], kv=to)
-    for at, (src, dst) in enumerate(((wg_h, pwg), (wu_h, pwu), (wd_h, pwd))):
+    for at, (src, dst) in enumerate(((wout_h, pwout), (wg_h, pwg), (wu_h, pwu), (wd_h, pwd))):
         send(src, dst, w_ssem.at[at], w_rsem.at[at], tp=other)
 
     def total_of(own, others):
@@ -191,12 +191,22 @@
         head_out * lax.rsqrt(jnp.mean(head_out * head_out, axis=1, keepdims=True) + EPSILON) * gain_rows
     )
     mixed = normed * jax.nn.sigmoid(outgate)
-    heads[me] = jnp.concatenate(
+    mixed_ref[...] = jnp.concatenate(
         [mixed[h * SEQ : (h + 1) * SEQ] for h in range(HEADS)], axis=1
     ).astype(BF16)
 
+    half, place = me // 8, me % 8
     for dz, dy in FAR:
-        send(heads.at[me], heads.at[me], c_ssem, c_rsem, kv=chip(dz, dy))
+        send(mixed_ref, heads.at[tp, place], c_ssem, c_rsem, kv=chip(dz, dy), tp=half)
+
+    @pl.when(tp == half)
+    def _():
+        heads[tp, place] = mixed_ref[...]
+
+    @pl.when(tp != half)
+    def _():
+        send(mixed_ref, heads.at[tp, place], c_ssem, c_rsem, tp=other)
+
     value_row = lax.broadcasted_iota(jnp.int32, (HEADS * SEQ, VD), 0)
     for pair in range(HEADS * SEQ):
         h, s = pair // SEQ, pair % SEQ
@@ -205,23 +215,33 @@
             forget_scale[pair : pair + 1, :] * mem[s, h] + input_scale[pair : pair + 1, :] * outer
         )
     ready("wout", "mgain")
-    wait_for(heads.at[0:15], c_rsem)
-    gathered = heads[...].astype(F32).reshape(KV * SEQ, HEADS * VD).astype(BF16)
-
-    half_send[...] = dot(gathered, wout[...]).astype(BF16)
-    send(half_send, half_recv, d_ssem, d_rsem, tp=other)
-    wait_for(half_recv, d_rsem)
-    branch = half_send[...].astype(F32) + half_recv[...].astype(F32)
-    residual = (tok[...].astype(F32) + branch).astype(BF16)
-    resid[...] = residual.astype(F32)
-    rows[me] = jnp.where(low, resid[0:64, :], resid[64:128, :]).astype(BF16)
+
+    @pl.when(tp == half)
+    def _():
+        wait_for(a1_recv.at[:, :, 0:1024], c_rsem)
+
+    @pl.when(tp != half)
+    def _():
+        wait_for(a1_send.at[:, :, 0:1024], c_rsem)
+
+    def group(at, w):
+        rows_of = heads[at].astype(F32).reshape(64, HEADS * VD).astype(BF16)
+        return dot(rows_of, w[...]).astype(BF16).astype(F32)
+
+    wait_for(pwout, w_rsem.at[0])
+    branch = group(tp, wout) + group(other, pwout)
+    own_rows = pl.ds(pl.multiple_of(tp * 64, 64), 64)
+    residual = (tok[own_rows, :].astype(F32) + branch).astype(BF16)
+    rows[me] = residual
+    resid[tp] = residual
 
     for dz, dy in FAR:
         send(rows.at[me], rows.at[me], e_ssem, e_rsem, kv=chip(dz, dy))
+    send(resid.at[tp], resid.at[tp], d_ssem, d_rsem, tp=other)
     ready("wg", "wu", "wd")
-    wait_for(pwg, w_rsem.at[0])
-    wait_for(pwu, w_rsem.at[1])
-    wait_for(pwd, w_rsem.at[2])
+    wait_for(pwg, w_rsem.at[1])
+    wait_for(pwu, w_rsem.at[2])
+    wait_for(pwd, w_rsem.at[3])
     wait_for(rows.at[0:15], e_rsem)
     whole = jnp.concatenate([rows[j].astype(F32) for j in range(KV)], axis=1)
     inverse_two = lax.rsqrt(jnp.mean(whole * whole, axis=1, keepdims=True) + EPSILON)
@@ -259,18 +279,28 @@
         for j in range(1, KV):
             total = total + down_recv[2 * j + core].astype(F32)
         pieces += [total, pltpu.roll(total, 64, 1)]
-    own = resid[...]
+    wait_for(resid.at[0], d_rsem)
+    own = resid[...].astype(F32).reshape(128, 128)
     own = jnp.where(low, own, pltpu.roll(own, 64, 1))
     summed = jnp.concatenate(pieces, axis=0) + own
     out_ref[...] = jnp.transpose(summed)[0:64, :].astype(BF16)
 
     wait_for(a1_recv, a_ssem.at[0])
     wait_for(a2_recv, a_ssem.at[1])
-    wait_for(pwg, w_ssem.at[0])
-    wait_for(pwu, w_ssem.at[1])
-    wait_for(pwd, w_ssem.at[2])
-    wait_for(heads.at[0:15], c_ssem)
-    wait_for(half_send, d_ssem)
+    wait_for(pwout, w_ssem.at[0])
+    wait_for(pwg, w_ssem.at[1])
+    wait_for(pwu, w_ssem.at[2])
+    wait_for(pwd, w_ssem.at[3])
+
+    @pl.when(tp == half)
+    def _():
+        wait_for(a1_recv.at[:, :, 0:1024], c_ssem)
+
+    @pl.when(tp != half)
+    def _():
+        wait_for(a1_send.at[:, :, 0:1024], c_ssem)
+
+    wait_for(resid.at[0], d_ssem)
     wait_for(rows.at[0:15], e_ssem)
     wait_for(down_recv.at[0:31], g_ssem)
 
@@ -310,20 +340,20 @@
             pltpu.VMEM(w_gate.shape[::-1], BF16),
             pltpu.VMEM(w_up.shape[::-1], BF16),
             pltpu.VMEM(w_down.shape, BF16),
+            pltpu.VMEM(w_out.shape, BF16),
             pltpu.VMEM((128, 128), F32),
             pltpu.VMEM((KV, SEQ, 1152), BF16),
             pltpu.VMEM((KV - 1, SEQ, 1152), BF16),
             pltpu.VMEM((KV, SEQ, 2048), BF16),
             pltpu.VMEM((KV - 1, SEQ, 2048), BF16),
             pltpu.VMEM((HEADS * SEQ, VD), F32),
-            pltpu.VMEM((KV, SEQ, HEADS * VD), BF16),
-            pltpu.VMEM((128, 128), BF16),
-            pltpu.VMEM((128, 128), BF16),
-            pltpu.VMEM((128, 128), F32),
+            pltpu.VMEM((SEQ, HEADS * VD), BF16),
+            pltpu.VMEM((2, KV // 2, SEQ, HEADS * VD), BF16),
+            pltpu.VMEM((2, 64, 128), BF16),
             pltpu.VMEM((KV, 64, 128), BF16),
             pltpu.VMEM((ROW, ROW, 2, 32, 128), BF16),
             pltpu.VMEM((2 * KV, 32, 128), BF16),
-            dma((len(args),)), dma((2,)), dma((2,)), dma((3,)), dma((3,)),
+            dma((len(args),)), dma((2,)), dma((2,)), dma((4,)), dma((4,)),
             dma, dma, dma, dma, dma, dma, dma, dma,
         ],
         compiler_params=pltpu.CompilerParams(

time: 41.5 us -> 40.8 us (0.983)
  Pallas kernels: 40.7 us -> 40.1 us
    pallas_call x1, Pallas kernels: 38.6 us -> 38 us  [body(): pl.pallas_call(layer, name='layer', out_shape=tuple((pltpu.VMEM(o.shape,...]
where the time goes in v3:
time: 40.8 us; the launch traced here: 40.7 us
  Pallas kernels  40.1 us (98%)
  between operations  0.65 us (2%)
    pallas_call x1, Pallas kernels, body(): pl.pallas_call(layer, name='layer', out_shape=tuple((pltpu.VMEM(o.shape,...  38 us
    pallas_call x1, Pallas kernels, body(): pl.pallas_call(finish, name='finish', out_shape=outs, in_specs=[pl.BlockS...  2.11 us

profile of v3, /device:TPU:1, one launch (start us, length us, event | category | flops | bytes accessed | tf_op | source)
XLA Modules:
  0.0 40.7 jit_solution(5016648116186160661)
XLA Ops:
  0.6 38.0 %layer.1 = (bf16[64,128]{1,0:T(8,128)(2,1)S(1)}, f32[8,4,128,256]{3,2,1,0:T(8,128)S(1)}, f32[8,4,128]{2,1,0:T(4,128)S(1)}, f32[4,8]{1,0:T(4,128)S(1)}) custom-call(bf16[128,128]{1,0:T(8,128)(2,1)} %tok_h.1, f32[1,128]{1,0:T(1,128)} %bitcast.14, bf16[128,512]{1,0:T(8,128)(2,1)} %wq_h.1, bf16[128,512]{1,0:T(8,128)(2,1)} %wk_h.1, bf16[128,1024]{1,0:T(8,128)(2,1)} %wv_h.1, ...), custom_call_target="tpu_custom_call" | custom-call | tf_op jit(solution)/shard_map/layer/pallas_call | solution.py:333
  38.6 2.1 %finish.1 = (bf16[64,128]{1,0:T(8,128)(2,1)}, f32[8,4,128,256]{3,2,1,0:T(8,128)}, f32[8,4,128]{2,1,0:T(4,128)}, f32[4,8]{1,0:T(4,128)}) custom-call(bf16[64,128]{1,0:T(8,128)(2,1)S(1)} %get-tuple-element.12.out, f32[8,4,128,256]{3,2,1,0:T(8,128)S(1)} %get-tuple-element.13.nmem, f32[8,4,128]{2,1,0:T(4,128)S(1)} %get-tuple-element.14.nnrm, ...), custom_call_target="tpu_custom_call" | custom-call | tf_op jit(solution)/shard_map/finish/pallas_call | solution.py:363

commit v4 on v3

--- a/solution.py
+++ b/solution.py
@@ -35,9 +35,9 @@
     wg_h, wu_h, wd_h,
     out_ref, nmem_ref, nnrm_ref, nstab_ref,
     tok, gain, wq, wk, wv, wo, wgates, bias, mem, nrm, stab, hgain, wout, mgain, wg, wu, wd,
-    pwg, pwu, pwd, pwout, ext, a1_send, a1_recv, a2_send, a2_recv, carried, mixed_ref, heads, resid, rows,
+    pwg, pwu, pwd, pwout, ext, y1_send, y1_recv, z1_send, z1_recv, y2_send, y2_recv, z2_send, z2_recv, o_send, o_recv, carried, mixed_ref, heads, resid, rows,
     down_send, down_recv,
-    in_sem, a_ssem, a_rsem, w_ssem, w_rsem, c_ssem, c_rsem, d_ssem, d_rsem, e_ssem, e_rsem, g_ssem, g_rsem,
+    in_sem, a_ssem, a_rsem, b_ssem, b_rsem, o_ssem, o_rsem, w_ssem, w_rsem, c_ssem, c_rsem, d_ssem, d_rsem, e_ssem, e_rsem, g_ssem, g_rsem,
 ):
     me = lax.axis_index("kv")
     tp = lax.axis_index("tp")
@@ -102,39 +102,81 @@
     extra = jnp.where(lane == 16, square, ext[...])
 
     def put(dst, at, value):
-        dst[:, :, at : at + value.shape[1]] = value.reshape(KV, SEQ, value.shape[1]).astype(BF16)
-
-    put(a1_send, 0, dot(scaled, wq[...]))
-    put(a1_send, 512, dot(scaled, wk[...]))
-    put(a1_send, 1024, extra)
+        dst[..., at : at + value.shape[1]] = value.reshape(*dst.shape[:-1], value.shape[1]).astype(BF16)
+
+    def first_step(at, ycols, zcols):
+        for step in (2, 1, 3):
+            column = (y + step) % ROW
+            send(
+                y1_send.at[:, column, :, ycols], y1_recv.at[step - 1, :, :, ycols], a_ssem.at[at], a_rsem.at[at],
+                kv=chip(0, step),
+            )
+            row = (z + step) % ROW
+            send(
+                z1_send.at[row, :, :, zcols], z1_recv.at[step - 1, :, :, zcols], a_ssem.at[at + 2], a_rsem.at[at + 2],
+                kv=chip(step, 0),
+            )
+
+    def second_step(at, ycols, zcols):
+        wait_for(y1_recv.at[:, :, :, ycols], a_rsem.at[at])
+        total = y1_send[:, y, :, ycols].astype(F32)
+        for slot in range(ROW - 1):
+            total = total + y1_recv[slot, :, :, ycols].astype(F32)
+        y2_send[:, :, ycols] = total.astype(BF16)
+        for step in (2, 1, 3):
+            row = (z + step) % ROW
+            send(
+                y2_send.at[row, :, ycols], y2_recv.at[step - 1, :, ycols], b_ssem.at[at], b_rsem.at[at],
+                kv=chip(step, 0),
+            )
+        wait_for(z1_recv.at[:, :, :, zcols], a_rsem.at[at + 2])
+        total = z1_send[z, :, :, zcols].astype(F32)
+        for slot in range(ROW - 1):
+            total = total + z1_recv[slot, :, :, zcols].astype(F32)
+        z2_send[:, :, zcols] = total.astype(BF16)
+        for step in (2, 1, 3):
+            column = (y + step) % ROW
+            send(
+                z2_send.at[column, :, zcols], z2_recv.at[step - 1, :, zcols], b_ssem.at[at + 2], b_rsem.at[at + 2],
+                kv=chip(0, step),
+            )
+
+    def arrived(at, send_buf, recv_buf, mine, cols):
+        wait_for(recv_buf.at[:, :, cols], b_rsem.at[at])
+        total = send_buf[mine, :, cols].astype(F32)
+        for slot in range(ROW - 1):
+            total = total + recv_buf[slot, :, cols].astype(F32)
+        return total
+
+    put(y1_send, 0, dot(scaled, wq[...]))
+    put(y1_send, 512, extra)
+    put(z1_send, 0, dot(scaled, wk[...]))
     pl.semaphore_wait(barrier, 2 * KV - 1)
+    early_y, early_z, late_y, late_z = pl.ds(0, 640), pl.ds(0, 512), pl.ds(640, 512), pl.ds(512, 512)
+    first_step(0, early_y, early_z)
+    ready("wv")
+    put(y1_send, 640, dot(scaled, wv[:, 0:512]))
+    put(z1_send, 512, dot(scaled, wv[:, 512:1024]))
+    first_step(1, late_y, late_z)
+    ready("wo")
+    put(o_send, 0, dot(scaled, wo[...]))
     for slot, (dz, dy) in enumerate(FAR):
         to = chip(dz, dy)
-        send(a1_send.at[to], a1_recv.at[slot], a_ssem.at[0], a_rsem.at[0], kv=to)
-    ready("wv", "wo")
-    put(a2_send, 0, dot(scaled, wv[...]))
-    put(a2_send, 1024, dot(scaled, wo[...]))
-    for slot, (dz, dy) in enumerate(FAR):
-        to = chip(dz, dy)
-        send(a2_send.at[to], a2_recv.at[slot], a_ssem.at[1], a_rsem.at[1], kv=to)
+        send(o_send.at[to // ROW, to % ROW], o_recv.at[slot], o_ssem, o_rsem, kv=to)
+    second_step(0, early_y, early_z)
+    second_step(1, late_y, late_z)
     for at, (src, dst) in enumerate(((wout_h, pwout), (wg_h, pwg), (wu_h, pwu), (wd_h, pwd))):
         send(src, dst, w_ssem.at[at], w_rsem.at[at], tp=other)
 
-    def total_of(own, others):
-        total = own[me].astype(F32)
-        for slot in range(KV - 1):
-            total = total + others[slot].astype(F32)
-        return total
-
     def by_head(value, width):
         return jnp.concatenate([value[:, h * width : (h + 1) * width] for h in range(HEADS)], axis=0)
 
-    wait_for(a1_recv, a_rsem.at[0])
-    first = total_of(a1_send, a1_recv)
-    inverse = lax.rsqrt(first[:, 1040:1041] * (1.0 / (KV * QK)) + EPSILON)
+    first = arrived(0, y2_send, y2_recv, z, early_y)
+    inverse = lax.rsqrt(first[:, 528:529] * (1.0 / (KV * QK)) + EPSILON)
     query = (first[:, 0:512] * inverse).astype(BF16).astype(F32)
-    key = (first[:, 512:1024] * (inverse * QK ** (-0.5))).astype(BF16).astype(F32)
-    gate_pre = first[:, 1024:1152] * inverse
+    key_sum = arrived(2, z2_send, z2_recv, y, early_z)
+    key = (key_sum * (inverse * QK ** (-0.5))).astype(BF16).astype(F32)
+    gate_pre = first[:, 512:640] * inverse
     low = tp == 0
     input_pre = jnp.where(low, gate_pre[:, 0:4], gate_pre[:, 4:8])
     forget_pre = jnp.where(low, gate_pre[:, 8:12], gate_pre[:, 12:16])
@@ -178,10 +220,10 @@
         carried[pair : pair + 1, 0:128] = low_half
         carried[pair : pair + 1, 128:256] = high_half
 
-    wait_for(a2_recv, a_rsem.at[1])
-    second = total_of(a2_send, a2_recv) * inverse
-    value_heads = by_head(second[:, 0:1024].astype(BF16).astype(F32), VD)
-    outgate = by_head(second[:, 1024:2048].astype(BF16).astype(F32), VD)
+    value_sum = jnp.concatenate(
+        [arrived(1, y2_send, y2_recv, z, late_y), arrived(3, z2_send, z2_recv, y, late_z)], axis=1
+    )
+    value_heads = by_head((value_sum * inverse).astype(BF16).astype(F32), VD)
     numerator = forget_scale * carried[...] + (input_scale * query_key) * value_heads
     head_out = numerator / jnp.maximum(jnp.abs(denominator), 1.0)
     gain_rows = jnp.concatenate(
@@ -190,6 +232,11 @@
     normed = (
         head_out * lax.rsqrt(jnp.mean(head_out * head_out, axis=1, keepdims=True) + EPSILON) * gain_rows
     )
+    wait_for(o_recv, o_rsem)
+    outgate_sum = o_send[z, y].astype(F32)
+    for slot in range(KV - 1):
+        outgate_sum = outgate_sum + o_recv[slot].astype(F32)
+    outgate = by_head((outgate_sum * inverse).astype(BF16).astype(F32), VD)
     mixed = normed * jax.nn.sigmoid(outgate)
     mixed_ref[...] = jnp.concatenate(
         [mixed[h * SEQ : (h + 1) * SEQ] for h in range(HEADS)], axis=1
@@ -218,11 +265,11 @@
 
     @pl.when(tp == half)
     def _():
-        wait_for(a1_recv.at[:, :, 0:1024], c_rsem)
+        wait_for(o_recv, c_rsem)
 
     @pl.when(tp != half)
     def _():
-        wait_for(a1_send.at[:, :, 0:1024], c_rsem)
+        wait_for(o_send, c_rsem)
 
     def group(at, w):
         rows_of = heads[at].astype(F32).reshape(64, HEADS * VD).astype(BF16)
@@ -285,8 +332,12 @@
     summed = jnp.concatenate(pieces, axis=0) + own
     out_ref[...] = jnp.transpose(summed)[0:64, :].astype(BF16)
 
-    wait_for(a1_recv, a_ssem.at[0])
-    wait_for(a2_recv, a_ssem.at[1])
+    for at, ycols, zcols in ((0, early_y, early_z), (1, late_y, late_z)):
+        wait_for(y1_recv.at[:, :, :, ycols], a_ssem.at[at])
+        wait_for(z1_recv.at[:, :, :, zcols], a_ssem.at[at + 2])
+        wait_for(y2_recv.at[:, :, ycols], b_ssem.at[at])
+        wait_for(z2_recv.at[:, :, zcols], b_ssem.at[at + 2])
+    wait_for(o_recv, o_ssem)
     wait_for(pwout, w_ssem.at[0])
     wait_for(pwg, w_ssem.at[1])
     wait_for(pwu, w_ssem.at[2])
@@ -294,11 +345,11 @@
 
     @pl.when(tp == half)
     def _():
-        wait_for(a1_recv.at[:, :, 0:1024], c_ssem)
+        wait_for(o_recv, c_ssem)
 
     @pl.when(tp != half)
     def _():
-        wait_for(a1_send.at[:, :, 0:1024], c_ssem)
+        wait_for(o_send, c_ssem)
 
     wait_for(resid.at[0], d_ssem)
     wait_for(rows.at[0:15], e_ssem)
@@ -342,10 +393,16 @@
             pltpu.VMEM(w_down.shape, BF16),
             pltpu.VMEM(w_out.shape, BF16),
             pltpu.VMEM((128, 128), F32),
-            pltpu.VMEM((KV, SEQ, 1152), BF16),
-            pltpu.VMEM((KV - 1, SEQ, 1152), BF16),
-            pltpu.VMEM((KV, SEQ, 2048), BF16),
-            pltpu.VMEM((KV - 1, SEQ, 2048), BF16),
+            pltpu.VMEM((ROW, ROW, SEQ, 1152), BF16),
+            pltpu.VMEM((ROW - 1, ROW, SEQ, 1152), BF16),
+            pltpu.VMEM((ROW, ROW, SEQ, 1024), BF16),
+            pltpu.VMEM((ROW - 1, ROW, SEQ, 1024), BF16),
+            pltpu.VMEM((ROW, SEQ, 1152), BF16),
+            pltpu.VMEM((ROW - 1, SEQ, 1152), BF16),
+            pltpu.VMEM((ROW, SEQ, 1024), BF16),
+            pltpu.VMEM((ROW - 1, SEQ, 1024), BF16),
+            pltpu.VMEM((ROW, ROW, SEQ, 1024), BF16),
+            pltpu.VMEM((KV - 1, SEQ, 1024), BF16),
             pltpu.VMEM((HEADS * SEQ, VD), F32),
             pltpu.VMEM((SEQ, HEADS * VD), BF16),
             pltpu.VMEM((2, KV // 2, SEQ, HEADS * VD), BF16),
@@ -353,7 +410,7 @@
             pltpu.VMEM((KV, 64, 128), BF16),
             pltpu.VMEM((ROW, ROW, 2, 32, 128), BF16),
             pltpu.VMEM((2 * KV, 32, 128), BF16),
-            dma((len(args),)), dma((2,)), dma((2,)), dma((4,)), dma((4,)),
+            dma((len(args),)), dma((4,)), dma((4,)), dma((4,)), dma((4,)), dma, dma, dma((4,)), dma((4,)),
             dma, dma, dma, dma, dma, dma, dma, dma,
         ],
         compiler_params=pltpu.CompilerParams(

time: 40.8 us -> 39.7 us (0.973)
  Pallas kernels: 40.1 us -> 38.9 us
    pallas_call x1, Pallas kernels: 38 us -> 36.8 us  [body(): pl.pallas_call(layer, name='layer', out_shape=tuple((pltpu.VMEM(o.shape,...]
where the time goes in v4:
time: 39.7 us; the launch traced here: 39.5 us
  Pallas kernels  38.9 us (98%)
  between operations  0.65 us (2%)
    pallas_call x1, Pallas kernels, body(): pl.pallas_call(layer, name='layer', out_shape=tuple((pltpu.VMEM(o.shape,...  36.8 us
    pallas_call x1, Pallas kernels, body(): pl.pallas_call(finish, name='finish', out_shape=outs, in_specs=[pl.BlockS...  2.11 us

profile of v4, /device:TPU:1, one launch (start us, length us, event | category | flops | bytes accessed | tf_op | source)
XLA Modules:
  0.0 39.5 jit_solution(5519445497315013238)
XLA Ops:
  0.6 36.8 %layer.1 = (bf16[64,128]{1,0:T(8,128)(2,1)S(1)}, f32[8,4,128,256]{3,2,1,0:T(8,128)S(1)}, f32[8,4,128]{2,1,0:T(4,128)S(1)}, f32[4,8]{1,0:T(4,128)S(1)}) custom-call(bf16[128,128]{1,0:T(8,128)(2,1)} %tok_h.1, f32[1,128]{1,0:T(1,128)} %bitcast.14, bf16[128,512]{1,0:T(8,128)(2,1)} %wq_h.1, bf16[128,512]{1,0:T(8,128)(2,1)} %wk_h.1, bf16[128,1024]{1,0:T(8,128)(2,1)} %wv_h.1, ...), custom_call_target="tpu_custom_call" | custom-call | tf_op jit(solution)/shard_map/layer/pallas_call | solution.py:384
  37.4 2.1 %finish.1 = (bf16[64,128]{1,0:T(8,128)(2,1)}, f32[8,4,128,256]{3,2,1,0:T(8,128)}, f32[8,4,128]{2,1,0:T(4,128)}, f32[4,8]{1,0:T(4,128)}) custom-call(bf16[64,128]{1,0:T(8,128)(2,1)S(1)} %get-tuple-element.12.out, f32[8,4,128,256]{3,2,1,0:T(8,128)S(1)} %get-tuple-element.13.nmem, f32[8,4,128]{2,1,0:T(4,128)S(1)} %get-tuple-element.14.nnrm, ...), custom_call_target="tpu_custom_call" | custom-call | tf_op jit(solution)/shard_map/finish/pallas_call | solution.py:420

commit v5 on v4

--- a/solution.py
+++ b/solution.py
@@ -37,7 +37,7 @@
     tok, gain, wq, wk, wv, wo, wgates, bias, mem, nrm, stab, hgain, wout, mgain, wg, wu, wd,
     pwg, pwu, pwd, pwout, ext, y1_send, y1_recv, z1_send, z1_recv, y2_send, y2_recv, z2_send, z2_recv, o_send, o_recv, carried, mixed_ref, heads, resid, rows,
     down_send, down_recv,
-    in_sem, a_ssem, a_rsem, b_ssem, b_rsem, o_ssem, o_rsem, w_ssem, w_rsem, c_ssem, c_rsem, d_ssem, d_rsem, e_ssem, e_rsem, g_ssem, g_rsem,
+    plane_sem, in_sem, a_ssem, a_rsem, b_ssem, b_rsem, o_ssem, o_rsem, w_ssem, w_rsem, c_ssem, c_rsem, d_ssem, d_rsem, e_ssem, e_rsem, g_ssem, g_rsem,
 ):
     me = lax.axis_index("kv")
     tp = lax.axis_index("tp")
@@ -48,11 +48,9 @@
         return ((z + dz) % ROW) * ROW + (y + dy) % ROW
 
     barrier = pltpu.get_barrier_semaphore()
-    for dz, dy in FAR:
-        for core in (tp, other):
-            pl.semaphore_signal(
-                barrier, inc=1, device_id={"kv": chip(dz, dy), "tp": core}, device_id_type=MESH
-            )
+    for step in (2, 1, 3):
+        pl.semaphore_signal(barrier, inc=1, device_id={"kv": chip(step, 0)}, device_id_type=MESH)
+        pl.semaphore_signal(barrier, inc=1, device_id={"kv": chip(0, step)}, device_id_type=MESH)
     pl.semaphore_signal(barrier, inc=1, device_id={"tp": other}, device_id_type=MESH)
 
     loads = {}
@@ -151,7 +149,9 @@
     put(y1_send, 0, dot(scaled, wq[...]))
     put(y1_send, 512, extra)
     put(z1_send, 0, dot(scaled, wk[...]))
-    pl.semaphore_wait(barrier, 2 * KV - 1)
+    pl.semaphore_wait(barrier, 2 * ROW - 1)
+    for step in (2, 1, 3):
+        pl.semaphore_signal(plane_sem, inc=1, device_id={"kv": chip(step, 0)}, device_id_type=MESH)
     early_y, early_z, late_y, late_z = pl.ds(0, 640), pl.ds(0, 512), pl.ds(640, 512), pl.ds(512, 512)
     first_step(0, early_y, early_z)
     ready("wv")
@@ -160,6 +160,7 @@
     first_step(1, late_y, late_z)
     ready("wo")
     put(o_send, 0, dot(scaled, wo[...]))
+    pl.semaphore_wait(plane_sem, ROW - 1)
     for slot, (dz, dy) in enumerate(FAR):
         to = chip(dz, dy)
         send(o_send.at[to // ROW, to % ROW], o_recv.at[slot], o_ssem, o_rsem, kv=to)
@@ -410,7 +411,7 @@
             pltpu.VMEM((KV, 64, 128), BF16),
             pltpu.VMEM((ROW, ROW, 2, 32, 128), BF16),
             pltpu.VMEM((2 * KV, 32, 128), BF16),
-            dma((len(args),)), dma((4,)), dma((4,)), dma((4,)), dma((4,)), dma, dma, dma((4,)), dma((4,)),
+            pltpu.SemaphoreType.REGULAR, dma((len(args),)), dma((4,)), dma((4,)), dma((4,)), dma((4,)), dma, dma, dma((4,)), dma((4,)),
             dma, dma, dma, dma, dma, dma, dma, dma,
         ],
         compiler_params=pltpu.CompilerParams(

time: 39.7 us -> 38 us (0.957)
  Pallas kernels: 38.9 us -> 37.3 us
    pallas_call x1, Pallas kernels: 36.8 us -> 35.2 us  [body(): pl.pallas_call(layer, name='layer', out_shape=tuple((pltpu.VMEM(o.shape,...]
where the time goes in v5:
time: 38 us; the launch traced here: 37.9 us
  Pallas kernels  37.3 us (98%)
  between operations  0.65 us (2%)
    pallas_call x1, Pallas kernels, body(): pl.pallas_call(layer, name='layer', out_shape=tuple((pltpu.VMEM(o.shape,...  35.2 us
    pallas_call x1, Pallas kernels, body(): pl.pallas_call(finish, name='finish', out_shape=outs, in_specs=[pl.BlockS...  2.11 us

profile of v5, /device:TPU:1, one launch (start us, length us, event | category | flops | bytes accessed | tf_op | source)
XLA Modules:
  0.0 37.9 jit_solution(9907120548128763113)
XLA Ops:
  0.6 35.2 %layer.1 = (bf16[64,128]{1,0:T(8,128)(2,1)S(1)}, f32[8,4,128,256]{3,2,1,0:T(8,128)S(1)}, f32[8,4,128]{2,1,0:T(4,128)S(1)}, f32[4,8]{1,0:T(4,128)S(1)}) custom-call(bf16[128,128]{1,0:T(8,128)(2,1)} %tok_h.1, f32[1,128]{1,0:T(1,128)} %bitcast.14, bf16[128,512]{1,0:T(8,128)(2,1)} %wq_h.1, bf16[128,512]{1,0:T(8,128)(2,1)} %wk_h.1, bf16[128,1024]{1,0:T(8,128)(2,1)} %wv_h.1, ...), custom_call_target="tpu_custom_call" | custom-call | tf_op jit(solution)/shard_map/layer/pallas_call | solution.py:385
  35.8 2.1 %finish.1 = (bf16[64,128]{1,0:T(8,128)(2,1)}, f32[8,4,128,256]{3,2,1,0:T(8,128)}, f32[8,4,128]{2,1,0:T(4,128)}, f32[4,8]{1,0:T(4,128)}) custom-call(bf16[64,128]{1,0:T(8,128)(2,1)S(1)} %get-tuple-element.12.out, f32[8,4,128,256]{3,2,1,0:T(8,128)S(1)} %get-tuple-element.13.nmem, f32[8,4,128]{2,1,0:T(4,128)S(1)} %get-tuple-element.14.nnrm, ...), custom_call_target="tpu_custom_call" | custom-call | tf_op jit(solution)/shard_map/finish/pallas_call | solution.py:421

commit v6 on v5

--- a/solution.py
+++ b/solution.py
@@ -280,26 +280,38 @@
     branch = group(tp, wout) + group(other, pwout)
     own_rows = pl.ds(pl.multiple_of(tp * 64, 64), 64)
     residual = (tok[own_rows, :].astype(F32) + branch).astype(BF16)
-    rows[me] = residual
+    rows[z, y] = residual
     resid[tp] = residual
 
-    for dz, dy in FAR:
-        send(rows.at[me], rows.at[me], e_ssem, e_rsem, kv=chip(dz, dy))
+    for dz in (2, 1, 3, 0):
+        for dy in (2, 1, 3, 0):
+            if (dz, dy) != (0, 0):
+                send(rows.at[z, y], rows.at[z, y], e_ssem, e_rsem.at[dz], kv=chip(dz, dy))
     send(resid.at[tp], resid.at[tp], d_ssem, d_rsem, tp=other)
     ready("wg", "wu", "wd")
     wait_for(pwg, w_rsem.at[1])
     wait_for(pwu, w_rsem.at[2])
     wait_for(pwd, w_rsem.at[3])
-    wait_for(rows.at[0:15], e_rsem)
-    whole = jnp.concatenate([rows[j].astype(F32) for j in range(KV)], axis=1)
-    inverse_two = lax.rsqrt(jnp.mean(whole * whole, axis=1, keepdims=True) + EPSILON)
-    mlp_in = (whole * inverse_two * mgain[...]).astype(BF16)
-
-    def hidden_of(gate_w, up_w):
-        return (jax.nn.silu(dot_rows(mlp_in, gate_w[...])) * dot_rows(mlp_in, up_w[...])).astype(BF16)
-
-    hidden_own = hidden_of(wg, wu)
-    hidden_other = hidden_of(pwg, pwu)
+
+    square_two, sums = None, None
+    for steps in ((0,), (1,), (3,), (2,)):
+        for dz in steps:
+            wait_for(rows.at[0, 0 : ROW - (dz == 0)], e_rsem.at[dz])
+        for dz in steps:
+            row = (z + ROW - dz) % ROW
+            span = pl.ds(pl.multiple_of(row * 512, 512), 512)
+            block = jnp.concatenate([rows[row, column].astype(F32) for column in range(ROW)], axis=1)
+            square = jnp.sum(block * block, axis=1, keepdims=True)
+            block = (block * mgain[:, span]).astype(BF16)
+            parts = [dot_rows(block, w[:, span]) for w in (wg, wu, pwg, pwu)]
+            if sums is None:
+                square_two, sums = square, parts
+            else:
+                square_two, sums = square_two + square, [a + b for a, b in zip(sums, parts)]
+    inverse_two = lax.rsqrt(square_two * (1.0 / (KV * QK)) + EPSILON)
+    gate_own, up_own, gate_other, up_other = [total * inverse_two for total in sums]
+    hidden_own = (jax.nn.silu(gate_own) * up_own).astype(BF16)
+    hidden_other = (jax.nn.silu(gate_other) * up_other).astype(BF16)
 
     lane_two = lax.broadcasted_iota(jnp.int32, (32, 128), 1)
     slot = me * 2 + tp
@@ -353,7 +365,8 @@
         wait_for(o_send, c_ssem)
 
     wait_for(resid.at[0], d_ssem)
-    wait_for(rows.at[0:15], e_ssem)
+    wait_for(rows.at[0:3], e_ssem)
+    wait_for(rows.at[0, 0:3], e_ssem)
     wait_for(down_recv.at[0:31], g_ssem)
 
 
@@ -408,11 +421,11 @@
             pltpu.VMEM((SEQ, HEADS * VD), BF16),
             pltpu.VMEM((2, KV // 2, SEQ, HEADS * VD), BF16),
             pltpu.VMEM((2, 64, 128), BF16),
-            pltpu.VMEM((KV, 64, 128), BF16),
+            pltpu.VMEM((ROW, ROW, 64, 128), BF16),
             pltpu.VMEM((ROW, ROW, 2, 32, 128), BF16),
             pltpu.VMEM((2 * KV, 32, 128), BF16),
             pltpu.SemaphoreType.REGULAR, dma((len(args),)), dma((4,)), dma((4,)), dma((4,)), dma((4,)), dma, dma, dma((4,)), dma((4,)),
-            dma, dma, dma, dma, dma, dma, dma, dma,
+            dma, dma, dma, dma, dma, dma((4,)), dma, dma,
         ],
         compiler_params=pltpu.CompilerParams(
             collective_id=0, has_side_effects=True, vmem_limit_bytes=40 * 1024 * 1024

time: 38 us -> 37.3 us (0.982)
  Pallas kernels: 37.3 us -> 36.5 us
    pallas_call x1, Pallas kernels: 35.2 us -> 34.4 us  [body(): pl.pallas_call(layer, name='layer', out_shape=tuple((pltpu.VMEM(o.shape,...]
where the time goes in v6:
time: 37.3 us; the launch traced here: 37.2 us
  Pallas kernels  36.5 us (98%)
  between operations  0.65 us (2%)
    pallas_call x1, Pallas kernels, body(): pl.pallas_call(layer, name='layer', out_shape=tuple((pltpu.VMEM(o.shape,...  34.4 us
    pallas_call x1, Pallas kernels, body(): pl.pallas_call(finish, name='finish', out_shape=outs, in_specs=[pl.BlockS...  2.11 us

profile of v6, /device:TPU:1, one launch (start us, length us, event | category | flops | bytes accessed | tf_op | source)
XLA Modules:
  0.0 37.2 jit_solution(18395582396335962181)
XLA Ops:
  0.6 34.4 %layer.1 = (bf16[64,128]{1,0:T(8,128)(2,1)S(1)}, f32[8,4,128,256]{3,2,1,0:T(8,128)S(1)}, f32[8,4,128]{2,1,0:T(4,128)S(1)}, f32[4,8]{1,0:T(4,128)S(1)}) custom-call(bf16[128,128]{1,0:T(8,128)(2,1)} %tok_h.1, f32[1,128]{1,0:T(1,128)} %bitcast.14, bf16[128,512]{1,0:T(8,128)(2,1)} %wq_h.1, bf16[128,512]{1,0:T(8,128)(2,1)} %wk_h.1, bf16[128,1024]{1,0:T(8,128)(2,1)} %wv_h.1, ...), custom_call_target="tpu_custom_call" | custom-call | tf_op jit(solution)/shard_map/layer/pallas_call | solution.py:398
  35.1 2.1 %finish.1 = (bf16[64,128]{1,0:T(8,128)(2,1)}, f32[8,4,128,256]{3,2,1,0:T(8,128)}, f32[8,4,128]{2,1,0:T(4,128)}, f32[4,8]{1,0:T(4,128)}) custom-call(bf16[64,128]{1,0:T(8,128)(2,1)S(1)} %get-tuple-element.12.out, f32[8,4,128,256]{3,2,1,0:T(8,128)S(1)} %get-tuple-element.13.nmem, f32[8,4,128]{2,1,0:T(4,128)S(1)} %get-tuple-element.14.nnrm, ...), custom_call_target="tpu_custom_call" | custom-call | tf_op jit(solution)/shard_map/finish/pallas_call | solution.py:434

commit v7 on v6

--- a/solution.py
+++ b/solution.py
@@ -33,10 +33,9 @@
 def layer(
     tok_h, gain_h, wq_h, wk_h, wv_h, wo_h, wgates_h, bias_h, mem_h, nrm_h, stab_h, hgain_h, wout_h, mgain_h,
     wg_h, wu_h, wd_h,
-    out_ref, nmem_ref, nnrm_ref, nstab_ref,
+    down_recv, resid, nmem_ref, nnrm_ref, nstab_ref,
     tok, gain, wq, wk, wv, wo, wgates, bias, mem, nrm, stab, hgain, wout, mgain, wg, wu, wd,
-    pwg, pwu, pwd, pwout, ext, y1_send, y1_recv, z1_send, z1_recv, y2_send, y2_recv, z2_send, z2_recv, o_send, o_recv, carried, mixed_ref, heads, resid, rows,
-    down_send, down_recv,
+    pwg, pwu, pwd, pwout, ext, y1_send, y1_recv, z1_send, z1_recv, y2_send, y2_recv, z2_send, z2_recv, o_send, o_recv, carried, mixed_ref, heads, rows, down_send,
     plane_sem, in_sem, a_ssem, a_rsem, b_ssem, b_rsem, o_ssem, o_rsem, w_ssem, w_rsem, c_ssem, c_rsem, d_ssem, d_rsem, e_ssem, e_rsem, g_ssem, g_rsem,
 ):
     me = lax.axis_index("kv")
@@ -333,17 +332,7 @@
                     )
     down_recv[slot] = down_send[0, y, tp]
     wait_for(down_recv.at[0:31], g_rsem)
-    pieces = []
-    for core in range(2):
-        total = down_recv[core].astype(F32)
-        for j in range(1, KV):
-            total = total + down_recv[2 * j + core].astype(F32)
-        pieces += [total, pltpu.roll(total, 64, 1)]
     wait_for(resid.at[0], d_rsem)
-    own = resid[...].astype(F32).reshape(128, 128)
-    own = jnp.where(low, own, pltpu.roll(own, 64, 1))
-    summed = jnp.concatenate(pieces, axis=0) + own
-    out_ref[...] = jnp.transpose(summed)[0:64, :].astype(BF16)
 
     for at, ycols, zcols in ((0, early_y, early_z), (1, late_y, late_z)):
         wait_for(y1_recv.at[:, :, :, ycols], a_ssem.at[at])
@@ -370,12 +359,23 @@
     wait_for(down_recv.at[0:31], g_ssem)
 
 
-def finish(out, nmem, nnrm, nstab, out_h, nmem_h, nnrm_h, nstab_h, sem):
+def finish(down_recv, resid, nmem, nnrm, nstab, out_h, nmem_h, nnrm_h, nstab_h, out, sem):
     copies = [(nmem.at[j], nmem_h.at[j]) for j in range(SEQ)]
     copies += [(nnrm, nnrm_h), (nstab, nstab_h), (out, out_h)]
     copies = [pltpu.make_async_copy(src, dst, sem.at[at]) for at, (src, dst) in enumerate(copies)]
-    for copy in copies:
+    for copy in copies[:-1]:
         copy.start()
+    pieces = []
+    for core in range(2):
+        total = down_recv[core].astype(F32)
+        for j in range(1, KV):
+            total = total + down_recv[2 * j + core].astype(F32)
+        pieces += [total, pltpu.roll(total, 64, 1)]
+    own = resid[...].astype(F32).reshape(128, 128)
+    own = jnp.where(lax.axis_index("tp") == 0, own, pltpu.roll(own, 64, 1))
+    summed = jnp.concatenate(pieces, axis=0) + own
+    out[...] = jnp.transpose(summed)[0:64, :].astype(BF16)
+    copies[-1].start()
     for copy in copies:
         copy.wait()
 
@@ -395,12 +395,13 @@
         jax.ShapeDtypeStruct(normalizer.shape, F32),
         jax.ShapeDtypeStruct((HEADS, SEQ), F32),
     )
+    parts = (jax.ShapeDtypeStruct((2 * KV, 32, 128), BF16), jax.ShapeDtypeStruct((2, 64, 128), BF16))
     results = pl.pallas_call(
         layer,
         name="layer",
-        out_shape=tuple(pltpu.VMEM(o.shape, o.dtype) for o in outs),
+        out_shape=tuple(pltpu.VMEM(o.shape, o.dtype) for o in parts + outs[1:]),
         in_specs=[pl.BlockSpec(memory_space=pltpu.HBM)] * len(args),
-        out_specs=[pl.BlockSpec(memory_space=pltpu.VMEM)] * 4,
+        out_specs=[pl.BlockSpec(memory_space=pltpu.VMEM)] * 5,
         scratch_shapes=copies + [
             pltpu.VMEM(w_gate.shape[::-1], BF16),
             pltpu.VMEM(w_up.shape[::-1], BF16),
@@ -420,10 +421,8 @@
             pltpu.VMEM((HEADS * SEQ, VD), F32),
             pltpu.VMEM((SEQ, HEADS * VD), BF16),
             pltpu.VMEM((2, KV // 2, SEQ, HEADS * VD), BF16),
-            pltpu.VMEM((2, 64, 128), BF16),
             pltpu.VMEM((ROW, ROW, 64, 128), BF16),
             pltpu.VMEM((ROW, ROW, 2, 32, 128), BF16),
-            pltpu.VMEM((2 * KV, 32, 128), BF16),
             pltpu.SemaphoreType.REGULAR, dma((len(args),)), dma((4,)), dma((4,)), dma((4,)), dma((4,)), dma, dma, dma((4,)), dma((4,)),
             dma, dma, dma, dma, dma, dma((4,)), dma, dma,
         ],
@@ -435,9 +434,9 @@
         finish,
         name="finish",
         out_shape=outs,
-        in_specs=[pl.BlockSpec(memory_space=pltpu.VMEM)] * 4,
+        in_specs=[pl.BlockSpec(memory_space=pltpu.VMEM)] * 5,
         out_specs=[pl.BlockSpec(memory_space=pltpu.HBM)] * 4,
-        scratch_shapes=[dma((SEQ + 3,))],
+        scratch_shapes=[pltpu.VMEM((64, 128), BF16), dma((SEQ + 3,))],
         compiler_params=pltpu.CompilerParams(vmem_limit_bytes=8 * 1024 * 1024),
     )(*results)
     return out.T, new_memory, new_normalizer, new_stabilizer.T

time: 37.3 us -> 37 us (level)
  no operation moved by 1% of the time
where the time goes in v7:
time: 37 us; the launch traced here: 36.9 us
  Pallas kernels  36.3 us (98%)
  between operations  0.65 us (2%)
    pallas_call x1, Pallas kernels, body(): pl.pallas_call(layer, name='layer', out_shape=tuple((pltpu.VMEM(o.shape,...  34.2 us
    pallas_call x1, Pallas kernels, body(): pl.pallas_call(finish, name='finish', out_shape=outs, in_specs=[pl.BlockS...  2.11 us

profile of v7, /device:TPU:1, one launch (start us, length us, event | category | flops | bytes accessed | tf_op | source)
XLA Modules:
  0.0 36.9 jit_solution(15425123546566195727)
XLA Ops:
  0.6 34.2 %layer.1 = (bf16[32,32,128]{2,1,0:T(8,128)(2,1)S(1)}, bf16[2,64,128]{2,1,0:T(8,128)(2,1)S(1)}, f32[8,4,128,256]{3,2,1,0:T(8,128)S(1)}, f32[8,4,128]{2,1,0:T(4,128)S(1)}, f32[4,8]{1,0:T(4,128)S(1)}) custom-call(bf16[128,128]{1,0:T(8,128)(2,1)} %tok_h.1, f32[1,128]{1,0:T(1,128)} %bitcast.14, bf16[128,512]{1,0:T(8,128)(2,1)} %wq_h.1, bf16[128,512]{1,0:T(8,128)(2,1)} %wk_h.1, ...), custom_call_target="tpu_custom_call" | custom-call | tf_op jit(solution)/shard_map/layer/pallas_call | solution.py:399
  34.8 2.1 %finish.1 = (bf16[64,128]{1,0:T(8,128)(2,1)}, f32[8,4,128,256]{3,2,1,0:T(8,128)}, f32[8,4,128]{2,1,0:T(4,128)}, f32[4,8]{1,0:T(4,128)}) custom-call(bf16[32,32,128]{2,1,0:T(8,128)(2,1)S(1)} %get-tuple-element.13.down_recv, bf16[2,64,128]{2,1,0:T(8,128)(2,1)S(1)} %get-tuple-element.14.resid, f32[8,4,128,256]{3,2,1,0:T(8,128)S(1)} %get-tuple-element.15.nmem, ...), custom_call_target="tpu_custom_call" | custom-call | tf_op jit(solution)/shard_map/finish/pallas_call | solution.py:433

commit v8 on v7

--- a/solution.py
+++ b/solution.py
@@ -40,11 +40,11 @@
 ):
     me = lax.axis_index("kv")
     tp = lax.axis_index("tp")
-    z, y = me // ROW, me % ROW
+    z, y = lax.div(me, ROW), lax.rem(me, ROW)
     other = 1 - tp
 
     def chip(dz, dy):
-        return ((z + dz) % ROW) * ROW + (y + dy) % ROW
+        return lax.rem(z + dz, ROW) * ROW + lax.rem(y + dy, ROW)
 
     barrier = pltpu.get_barrier_semaphore()
     for step in (2, 1, 3):
@@ -103,12 +103,12 @@
 
     def first_step(at, ycols, zcols):
         for step in (2, 1, 3):
-            column = (y + step) % ROW
+            column = lax.rem(y + step, ROW)
             send(
                 y1_send.at[:, column, :, ycols], y1_recv.at[step - 1, :, :, ycols], a_ssem.at[at], a_rsem.at[at],
                 kv=chip(0, step),
             )
-            row = (z + step) % ROW
+            row = lax.rem(z + step, ROW)
             send(
                 z1_send.at[row, :, :, zcols], z1_recv.at[step - 1, :, :, zcols], a_ssem.at[at + 2], a_rsem.at[at + 2],
                 kv=chip(step, 0),
@@ -121,7 +121,7 @@
             total = total + y1_recv[slot, :, :, ycols].astype(F32)
         y2_send[:, :, ycols] = total.astype(BF16)
         for step in (2, 1, 3):
-            row = (z + step) % ROW
+            row = lax.rem(z + step, ROW)
             send(
                 y2_send.at[row, :, ycols], y2_recv.at[step - 1, :, ycols], b_ssem.at[at], b_rsem.at[at],
                 kv=chip(step, 0),
@@ -132,7 +132,7 @@
             total = total + z1_recv[slot, :, :, zcols].astype(F32)
         z2_send[:, :, zcols] = total.astype(BF16)
         for step in (2, 1, 3):
-            column = (y + step) % ROW
+            column = lax.rem(y + step, ROW)
             send(
                 z2_send.at[column, :, zcols], z2_recv.at[step - 1, :, zcols], b_ssem.at[at + 2], b_rsem.at[at + 2],
                 kv=chip(0, step),
@@ -160,9 +160,9 @@
     ready("wo")
     put(o_send, 0, dot(scaled, wo[...]))
     pl.semaphore_wait(plane_sem, ROW - 1)
-    for slot, (dz, dy) in enumerate(FAR):
+    for slot, (dz, dy) in enumerate([(a, b) for a in (2, 1, 3, 0) for b in (2, 1, 3, 0) if (a, b) != (0, 0)]):
         to = chip(dz, dy)
-        send(o_send.at[to // ROW, to % ROW], o_recv.at[slot], o_ssem, o_rsem, kv=to)
+        send(o_send.at[lax.div(to, ROW), lax.rem(to, ROW)], o_recv.at[slot], o_ssem, o_rsem, kv=to)
     second_step(0, early_y, early_z)
     second_step(1, late_y, late_z)
     for at, (src, dst) in enumerate(((wout_h, pwout), (wg_h, pwg), (wu_h, pwu), (wd_h, pwd))):
@@ -242,8 +242,8 @@
         [mixed[h * SEQ : (h + 1) * SEQ] for h in range(HEADS)], axis=1
     ).astype(BF16)
 
-    half, place = me // 8, me % 8
-    for dz, dy in FAR:
+    half, place = lax.div(me, 8), lax.rem(me, 8)
+    for dz, dy in [(a, b) for a in (2, 1, 3, 0) for b in (2, 1, 3, 0) if (a, b) != (0, 0)]:
         send(mixed_ref, heads.at[tp, place], c_ssem, c_rsem, kv=chip(dz, dy), tp=half)
 
     @pl.when(tp == half)
@@ -297,7 +297,7 @@
         for dz in steps:
             wait_for(rows.at[0, 0 : ROW - (dz == 0)], e_rsem.at[dz])
         for dz in steps:
-            row = (z + ROW - dz) % ROW
+            row = lax.rem(z + ROW - dz, ROW)
             span = pl.ds(pl.multiple_of(row * 512, 512), 512)
             block = jnp.concatenate([rows[row, column].astype(F32) for column in range(ROW)], axis=1)
             square = jnp.sum(block * block, axis=1, keepdims=True)
@@ -315,7 +315,7 @@
     lane_two = lax.broadcasted_iota(jnp.int32, (32, 128), 1)
     slot = me * 2 + tp
     for dz in (2, 1, 3, 0):
-        cols = pl.ds(pl.multiple_of(((z + dz) % ROW) * 512, 512), 512)
+        cols = pl.ds(pl.multiple_of(lax.rem(z + dz, ROW) * 512, 512), 512)
         part = dot(hidden_own, wd[:, cols]) + dot(hidden_other, pwd[:, cols])
         for at in range(ROW):
             top = part[0:32, at * 128 : (at + 1) * 128]
@@ -323,7 +323,7 @@
             down_send[dz, at, 0] = jnp.where(lane_two < 64, top, pltpu.roll(bottom, 64, 1)).astype(BF16)
             down_send[dz, at, 1] = jnp.where(lane_two < 64, pltpu.roll(top, 64, 1), bottom).astype(BF16)
         for dy in (2, 1, 3, 0):
-            column = (y + dy) % ROW
+            column = lax.rem(y + dy, ROW)
             for core in (tp, other):
                 if (dz, dy) != (0, 0) or core is other:
                     send(

time: 37 us -> 36.8 us (level)
  no operation moved by 1% of the time
where the time goes in v8:
time: 36.8 us; the launch traced here: 36.7 us
  Pallas kernels  36 us (98%)
  between operations  0.65 us (2%)
    pallas_call x1, Pallas kernels, body(): pl.pallas_call(layer, name='layer', out_shape=tuple((pltpu.VMEM(o.shape,...  33.9 us
    pallas_call x1, Pallas kernels, body(): pl.pallas_call(finish, name='finish', out_shape=outs, in_specs=[pl.BlockS...  2.11 us

profile of v8, /device:TPU:1, one launch (start us, length us, event | category | flops | bytes accessed | tf_op | source)
XLA Modules:
  0.0 36.7 jit_solution(740255281215080966)
XLA Ops:
  0.6 33.9 %layer.1 = (bf16[32,32,128]{2,1,0:T(8,128)(2,1)S(1)}, bf16[2,64,128]{2,1,0:T(8,128)(2,1)S(1)}, f32[8,4,128,256]{3,2,1,0:T(8,128)S(1)}, f32[8,4,128]{2,1,0:T(4,128)S(1)}, f32[4,8]{1,0:T(4,128)S(1)}) custom-call(bf16[128,128]{1,0:T(8,128)(2,1)} %tok_h.1, f32[1,128]{1,0:T(1,128)} %bitcast.14, bf16[128,512]{1,0:T(8,128)(2,1)} %wq_h.1, bf16[128,512]{1,0:T(8,128)(2,1)} %wk_h.1, ...), custom_call_target="tpu_custom_call" | custom-call | tf_op jit(solution)/shard_map/layer/pallas_call | solution.py:399
  34.5 2.1 %finish.1 = (bf16[64,128]{1,0:T(8,128)(2,1)}, f32[8,4,128,256]{3,2,1,0:T(8,128)}, f32[8,4,128]{2,1,0:T(4,128)}, f32[4,8]{1,0:T(4,128)}) custom-call(bf16[32,32,128]{2,1,0:T(8,128)(2,1)S(1)} %get-tuple-element.13.down_recv, bf16[2,64,128]{2,1,0:T(8,128)(2,1)S(1)} %get-tuple-element.14.resid, f32[8,4,128,256]{3,2,1,0:T(8,128)S(1)} %get-tuple-element.15.nmem, ...), custom_call_target="tpu_custom_call" | custom-call | tf_op jit(solution)/shard_map/finish/pallas_call | solution.py:433

commit v9 on v8

--- a/solution.py
+++ b/solution.py
@@ -314,7 +314,7 @@
 
     lane_two = lax.broadcasted_iota(jnp.int32, (32, 128), 1)
     slot = me * 2 + tp
-    for dz in (2, 1, 3, 0):
+    for dz in (1, 3, 2, 0):
         cols = pl.ds(pl.multiple_of(lax.rem(z + dz, ROW) * 512, 512), 512)
         part = dot(hidden_own, wd[:, cols]) + dot(hidden_other, pwd[:, cols])
         for at in range(ROW):

time: 36.8 us -> 37.3 us (1.014)
  Pallas kernels: 36 us -> 36.6 us
    pallas_call x1, Pallas kernels: 33.9 us -> 34.5 us  [body(): pl.pallas_call(layer, name='layer', out_shape=tuple((pltpu.VMEM(o.shape,...]
where the time goes in v9:
time: 37.3 us; the launch traced here: 37.2 us
  Pallas kernels  36.6 us (98%)
  between operations  0.65 us (2%)
    pallas_call x1, Pallas kernels, body(): pl.pallas_call(layer, name='layer', out_shape=tuple((pltpu.VMEM(o.shape,...  34.5 us
    pallas_call x1, Pallas kernels, body(): pl.pallas_call(finish, name='finish', out_shape=outs, in_specs=[pl.BlockS...  2.11 us

profile of v9, /device:TPU:1, one launch (start us, length us, event | category | flops | bytes accessed | tf_op | source)
XLA Modules:
  0.0 37.2 jit_solution(8772739181838657547)
XLA Ops:
  0.6 34.5 %layer.1 = (bf16[32,32,128]{2,1,0:T(8,128)(2,1)S(1)}, bf16[2,64,128]{2,1,0:T(8,128)(2,1)S(1)}, f32[8,4,128,256]{3,2,1,0:T(8,128)S(1)}, f32[8,4,128]{2,1,0:T(4,128)S(1)}, f32[4,8]{1,0:T(4,128)S(1)}) custom-call(bf16[128,128]{1,0:T(8,128)(2,1)} %tok_h.1, f32[1,128]{1,0:T(1,128)} %bitcast.14, bf16[128,512]{1,0:T(8,128)(2,1)} %wq_h.1, bf16[128,512]{1,0:T(8,128)(2,1)} %wk_h.1, ...), custom_call_target="tpu_custom_call" | custom-call | tf_op jit(solution)/shard_map/layer/pallas_call | solution.py:399
  35.1 2.1 %finish.1 = (bf16[64,128]{1,0:T(8,128)(2,1)}, f32[8,4,128,256]{3,2,1,0:T(8,128)}, f32[8,4,128]{2,1,0:T(4,128)}, f32[4,8]{1,0:T(4,128)}) custom-call(bf16[32,32,128]{2,1,0:T(8,128)(2,1)S(1)} %get-tuple-element.13.down_recv, bf16[2,64,128]{2,1,0:T(8,128)(2,1)S(1)} %get-tuple-element.14.resid, f32[8,4,128,256]{3,2,1,0:T(8,128)S(1)} %get-tuple-element.15.nmem, ...), custom_call_target="tpu_custom_call" | custom-call | tf_op jit(solution)/shard_map/finish/pallas_call | solution.py:433
